TPU v7x, 512 devices: a 8x2x16 block of a 8x16x16 slice. The times are simulated.
512 devices in a mesh: grp: 2 (over y), tp: 16 (over z), dp: 16 (over x, core).
Axes of the slice: x: 8, y: 2, z: 16, core: 2. Of those that a mesh axis runs over, the one named last changes fastest.
The devices are a block of a 8x16x16 slice.
Arguments:
- tokens: bfloat16 [512, 2048], P(('grp', 'tp'), 'dp'), parts along dimension 0, may hold values from -200 to 200
- norm_gain: bfloat16 [2, 2048], P(None, 'dp'), may hold values from 0.099609375 to 1.8984375
- w_z: bfloat16 [2, 2048, 4096], P(None, 'dp', 'tp'), may hold values from -0.125 to 0.125
- w_x: bfloat16 [2, 2048, 4096], P(None, 'dp', 'tp'), may hold values from -0.125 to 0.125
- w_b: bfloat16 [2, 2048, 1024], P(None, 'dp', 'tp'), may hold values from -0.125 to 0.125
- w_c: bfloat16 [2, 2048, 1024], P(None, 'dp', 'tp'), may hold values from -0.125 to 0.125
- w_dt: bfloat16 [2, 2048, 64], P(None, 'dp'), may hold values from -0.125 to 0.125
- conv_x: bfloat16 [2, 4, 4096], P(None, None, 'tp'), may hold values from -3 to 3
- conv_b: bfloat16 [2, 4, 1024], P(None, None, 'tp'), may hold values from -3 to 3
- conv_c: bfloat16 [2, 4, 1024], P(None, None, 'tp'), may hold values from -3 to 3
- dt_bias: float32 [2, 64], P(None, 'tp'), may hold values from -3 to 0.5
- a_log: float32 [2, 64], P(None, 'tp'), may hold values from 0 to 2.5
- d_skip: float32 [2, 64], P(None, 'tp'), may hold values from 0.5 to 2
- out_gain: bfloat16 [2, 4096], P(None, 'tp'), may hold values from 0.099609375 to 1.8984375
- w_out: bfloat16 [2, 4096, 2048], P(None, 'tp', 'dp'), may hold values from -0.09375 to 0.09375
- ssm_state: float32 [2, 512, 64, 64, 64], P(None, ('grp', 'dp'), 'tp'), parts along dimension 1, may hold values from -3 to 3
- state_x: bfloat16 [2, 512, 3, 4096], P(None, ('grp', 'dp'), None, 'tp'), parts along dimension 1, may hold values from -6 to 6
- state_b: bfloat16 [2, 512, 3, 1024], P(None, ('grp', 'dp'), None, 'tp'), parts along dimension 1, may hold values from -6 to 6
- state_c: bfloat16 [2, 512, 3, 1024], P(None, ('grp', 'dp'), None, 'tp'), parts along dimension 1, may hold values from -6 to 6
Outputs:
- residual: bfloat16 [512, 2048], P(('grp', 'tp'), 'dp'), parts along dimension 0
- ssm_next: float32 [2, 512, 64, 64, 64], P(None, ('grp', 'dp'), 'tp'), parts along dimension 1
- next_x: bfloat16 [2, 512, 3, 4096], P(None, ('grp', 'dp'), None, 'tp'), parts along dimension 1
- next_b: bfloat16 [2, 512, 3, 1024], P(None, ('grp', 'dp'), None, 'tp'), parts along dimension 1
- next_c: bfloat16 [2, 512, 3, 1024], P(None, ('grp', 'dp'), None, 'tp'), parts along dimension 1
There are 2 independent parts, one for each index of `grp`. A program takes and returns all parts, laid end to end along the dimension named above; an argument that names none is the same for every part. Nothing has to cross between parts.
All inputs are finite; a program needn't handle non-finite values.
Results may differ from a plain program's by a relative error of at most 0.0095.
Values may be sent and summed in bfloat16 or wider, within the bound.
A program may use at most 64 MiB of HBM per device.

v0:
```python
import jax
import jax.numpy as jnp
from jax import lax
from jax.sharding import PartitionSpec as P

HEAD_DIM = 64
STATE = 64


EPSILON = 1e-05


def laid_out(blocks, dim):
    blocks = jnp.moveaxis(blocks, 0, dim)
    dims = blocks.shape
    return blocks.reshape(*dims[:dim], dims[dim] * dims[dim + 1], *dims[dim + 2 :])


def copy_for_each(array, axis):
    copies = jnp.broadcast_to(array, (lax.axis_size(axis), *array.shape))
    return lax.all_to_all(copies, axis, split_axis=0, concat_axis=0, tiled=True)


def gather_directly(array, axis, dim):
    return laid_out(copy_for_each(array, axis), dim)


def cut_along(array, dim, length):
    before, after = (array.shape[:dim], array.shape[dim + 1 :])
    return jnp.moveaxis(array.reshape(*before, length, -1, *after), dim, 0)


def summed_on_arrival(array, axis, dim):
    blocks = cut_along(array, dim, lax.axis_size(axis))
    arrived = lax.all_to_all(blocks, axis, split_axis=0, concat_axis=0, tiled=True)
    return arrived.sum(axis=0)


def convolve(history, latest, weight):
    window = jnp.concatenate([history, latest[:, None, :]], axis=1)
    summed = jnp.sum(window.astype(jnp.float32) * weight.astype(jnp.float32)[None], axis=1)
    return (jax.nn.silu(summed), window[:, 1:])


def mixer(gate_in, conv_xv, conv_bv, conv_cv, step_raw, bias, log_rate, skip, gain, state_prev):
    seq_count = conv_xv.shape[0]
    heads_here = step_raw.shape[1]
    group_count = conv_bv.shape[1] // STATE
    per_group = heads_here // group_count
    step_size = jax.nn.softplus(step_raw + bias)
    decay_rate = jnp.exp(-step_size * jnp.exp(log_rate))
    x_heads = conv_xv.reshape(seq_count, group_count, per_group, HEAD_DIM)
    b_state = conv_bv.reshape(seq_count, group_count, 1, 1, STATE)
    c_state = conv_cv.reshape(seq_count, group_count, 1, 1, STATE)
    step_heads = step_size.reshape(seq_count, group_count, per_group, 1)
    decay_heads = decay_rate.reshape(seq_count, group_count, per_group, 1, 1)
    previous = state_prev.reshape(seq_count, group_count, per_group, HEAD_DIM, STATE)
    state_next = decay_heads * previous + (step_heads * x_heads)[..., None] * b_state
    readout = (
        jnp.sum(state_next * c_state, axis=-1)
        + skip.reshape(1, group_count, per_group, 1) * x_heads
    )
    gated_out = readout.reshape(seq_count, group_count, -1) * jax.nn.silu(
        gate_in.astype(jnp.float32)
    ).reshape(seq_count, group_count, -1)
    normed = gated_out * lax.rsqrt(
        jnp.mean(gated_out * gated_out, axis=-1, keepdims=True) + EPSILON
    )
    mixed_out = (normed.reshape(seq_count, -1) * gain.astype(jnp.float32)).astype(jnp.bfloat16)
    return (mixed_out, state_next.reshape(seq_count, heads_here, HEAD_DIM, STATE))


def body(
    tokens,
    norm_gain,
    w_z,
    w_x,
    w_b,
    w_c,
    w_dt,
    conv_x,
    conv_b,
    conv_c,
    dt_bias,
    a_log,
    d_skip,
    out_gain,
    w_out,
    ssm_state,
    state_x,
    state_b,
    state_c,
):
    dp_size = lax.axis_size("dp")
    residual = tokens
    states, saved_x, saved_b, saved_c = ([], [], [], [])
    width_z = w_z.shape[2]
    width_b = w_b.shape[2]
    width_dt = w_dt.shape[2]
    for layer_index in range(w_z.shape[0]):
        gathered_rows = gather_directly(residual, "tp", 0)
        seq_dev = gathered_rows.shape[0] // dp_size
        features = gathered_rows.shape[1] * dp_size
        widened = gathered_rows.astype(jnp.float32)
        squares = jnp.sum(widened * widened, axis=1)
        scaled = (widened * norm_gain[layer_index].astype(jnp.float32)).astype(jnp.bfloat16)
        matrices = (
            w_z[layer_index],
            w_x[layer_index],
            w_b[layer_index],
            w_c[layer_index],
            w_dt[layer_index],
        )
        pieces = 1
        piece_rows = seq_dev // pieces
        rows_piece = scaled.reshape(dp_size, seq_dev, -1).reshape(dp_size * piece_rows, -1)
        columns = [
            jnp.dot(rows_piece, matrix, preferred_element_type=jnp.float32) for matrix in matrices
        ]
        columns.append(squares.reshape(dp_size, seq_dev).reshape(-1, 1))
        merged_terms = jnp.concatenate(columns, axis=1)
        collected = summed_on_arrival(merged_terms, "dp", 0)
        total_squares = collected[:, 2 * width_z + 2 * width_b + width_dt]
        row_scale = lax.rsqrt(total_squares / features + EPSILON)[:, None]
        gate_in = (collected[:, 0:width_z] * row_scale).astype(jnp.bfloat16)
        x_in = (collected[:, width_z : 2 * width_z] * row_scale).astype(jnp.bfloat16)
        b_in = (collected[:, 2 * width_z : 2 * width_z + width_b] * row_scale).astype(jnp.bfloat16)
        c_in = (collected[:, 2 * width_z + width_b : 2 * width_z + 2 * width_b] * row_scale).astype(
            jnp.bfloat16
        )
        step_all = (
            collected[:, 2 * width_z + 2 * width_b : 2 * width_z + 2 * width_b + width_dt]
            * row_scale
        )
        heads_here = dt_bias.shape[1]
        step_raw = lax.dynamic_slice_in_dim(
            step_all, lax.axis_index("tp") * heads_here, heads_here, 1
        )
        conv_xv, kept_x = convolve(state_x[layer_index], x_in, conv_x[layer_index])
        conv_bv, kept_b = convolve(state_b[layer_index], b_in, conv_b[layer_index])
        conv_cv, kept_c = convolve(state_c[layer_index], c_in, conv_c[layer_index])
        mixed_out, state_next = mixer(
            gate_in,
            conv_xv,
            conv_bv,
            conv_cv,
            step_raw,
            dt_bias[layer_index],
            a_log[layer_index],
            d_skip[layer_index],
            out_gain[layer_index],
            ssm_state[layer_index],
        )
        all_mixed = gather_directly(mixed_out, "dp", 0)
        weight_out = w_out[layer_index]

        def head_term(first_row, row_count, source=all_mixed, matrix=weight_out):
            return jnp.dot(source, matrix, preferred_element_type=jnp.float32)

        projected = summed_on_arrival(
            head_term(jnp.int32(0), residual.shape[0] * lax.axis_size("tp")), "tp", 0
        )
        residual = (residual.astype(jnp.float32) + projected).astype(jnp.bfloat16)
        states.append(state_next)
        saved_x.append(kept_x)
        saved_b.append(kept_b)
        saved_c.append(kept_c)
    return (residual, jnp.stack(states), jnp.stack(saved_x), jnp.stack(saved_b), jnp.stack(saved_c))


def solution(mesh):
    placed = (
        P(("grp", "tp"), "dp"),
        P(None, "dp"),
        P(None, "dp", "tp"),
        P(None, "dp", "tp"),
        P(None, "dp", "tp"),
        P(None, "dp", "tp"),
        P(None, "dp", None),
        P(None, None, "tp"),
        P(None, None, "tp"),
        P(None, None, "tp"),
        P(None, "tp"),
        P(None, "tp"),
        P(None, "tp"),
        P(None, "tp"),
        P(None, "tp", "dp"),
        P(None, ("grp", "dp"), "tp", None, None),
        P(None, ("grp", "dp"), None, "tp"),
        P(None, ("grp", "dp"), None, "tp"),
        P(None, ("grp", "dp"), None, "tp"),
    )
    return jax.shard_map(
        body,
        mesh=mesh,
        in_specs=placed,
        out_specs=(
            P(("grp", "tp"), "dp"),
            P(None, ("grp", "dp"), "tp", None, None),
            P(None, ("grp", "dp"), None, "tp"),
            P(None, ("grp", "dp"), None, "tp"),
            P(None, ("grp", "dp"), None, "tp"),
        ),
        check_vma=False,
    )
```

profile of v0, /device:TPU:65, one launch (start us, length us, event | category | flops | bytes accessed | tf_op | source)
XLA Modules:
  0.0 209.3 jit_solution(11287917767721816587)
XLA Ops:
  0.6 1.3 broadcast_in_dim.20
  2.0 44.2 %all-to-all-start = ((bf16[16,16,128]{2,1,0:T(8,128)(2,1)}), bf16[16,16,128]{2,1,0:T(8,128)(2,1)S(1)}, u32[]{:S(2)}, u32[]{:S(2)}) async-start(bf16[16,16,128]{2,1,0:T(8,128)(2,1)} %broadcast_in_dim.20), calls=%async_computation | async-start | bytes 131072 | tf_op jit(solution)/shard_map/all_to_all | solution.py:21
  46.2 0.8 slice_convert_fusion
  46.9 0.7 bitcast_convert_fusion.6
  47.7 0.8 exponential_bitcast_fusion
  48.4 9.1 %all-to-all-done = bf16[16,16,128]{2,1,0:T(8,128)(2,1)S(1)} async-done(((bf16[16,16,128]{2,1,0:T(8,128)(2,1)}), bf16[16,16,128]{2,1,0:T(8,128)(2,1)S(1)}, u32[]{:S(2)}, u32[]{:S(2)}) %all-to-all-start) | async-done | bytes 65568 | tf_op jit(solution)/shard_map/all_to_all | solution.py:21
  57.5 0.1 fusion.7
  57.7 0.2 copy.24
  57.8 0.9 fusion.40
  58.7 0.9 fusion.38
  59.6 0.9 fusion.36
  60.5 1.0 fusion.18
  61.6 1.0 fusion.20
  62.6 1.0 concatenate.31
  63.6 9.5 %all-to-all-start.1 = ((f32[16,16,705]{2,1,0:T(8,128)}), f32[16,16,705]{2,1,0:T(8,128)S(1)}, u32[]{:S(2)}, u32[]{:S(2)}) async-start(f32[16,16,705]{2,1,0:T(8,128)} %concatenate.31), calls=%async_computation.1 | async-start | bytes 1572864 | tf_op jit(solution)/shard_map/all_to_all | solution.py:35
  73.4 22.4 %all-to-all-done.1 = f32[16,16,705]{2,1,0:T(8,128)S(1)} async-done(((f32[16,16,705]{2,1,0:T(8,128)}), f32[16,16,705]{2,1,0:T(8,128)S(1)}, u32[]{:S(2)}, u32[]{:S(2)}) %all-to-all-start.1) | async-done | bytes 721952 | tf_op jit(solution)/shard_map/all_to_all | solution.py:35
  95.9 0.2 fusion.95
  96.7 2.7 %fusion.5 = f32[16,4,64]{2,1,0:T(4,128)S(1)} fusion(f32[2,16,4,64,64]{4,3,2,1,0:T(8,128)} %param.34, f32[16,64]{1,0:T(8,128)S(1)} %divide_multiply_fusion.4, f32[16,64]{1,0:T(8,128)S(1)} %divide_multiply_fusion.5, f32[16,4,64]{2,1,0:T(4,128)S(1)} %fusion.45, f32[16,4]{1,0:T(8,128)S(1)} %get-tuple-element.11), kind=kLoop, calls=%fused_computation.8 | loop fusion | flops 1306624 | bytes 1089792 | tf_op jit(solution)/shard_map/reduce_sum | solution.py:60
  99.4 0.2 multiply_reduce_fusion.7
  99.7 11.8 %all_to_all.40 = bf16[16,16,256]{2,1,0:T(8,128)(2,1)S(1)} all-to-all(bf16[16,16,256]{2,1,0:T(8,128)(2,1)S(1)} %broadcast_in_dim.24), channel_id=1, replica_groups=mesh['grp'=2,'tp'=16,'dp'=16] {'dp'}, dimensions={0} | all-to-all | bytes 262144 | tf_op jit(solution)/shard_map/all_to_all | solution.py:21
  111.5 0.2 fusion.16
  111.7 15.4 %all_to_all.41 = f32[16,16,128]{2,1,0:T(8,128)S(1)} all-to-all(f32[16,16,128]{2,1,0:T(8,128)S(1)} %fusion.16), channel_id=1, replica_groups=mesh['grp'=2,'tp'=16,'dp'=16] {'tp'}, dimensions={0} | all-to-all | bytes 262144 | tf_op jit(solution)/shard_map/all_to_all | solution.py:35
  127.1 17.4 %all_to_all.42 = bf16[16,16,128]{2,1,0:T(8,128)(2,1)S(1)} all-to-all(bf16[16,16,128]{2,1,0:T(8,128)(2,1)S(1)} %broadcast_in_dim.25), channel_id=1, replica_groups=mesh['grp'=2,'tp'=16,'dp'=16] {'tp'}, dimensions={0} | all-to-all | bytes 131072 | tf_op jit(solution)/shard_map/all_to_all | solution.py:21
  144.5 0.1 fusion.9
  144.6 0.2 copy.25
  144.8 0.1 fusion.32
  144.9 0.1 fusion.30
  145.1 0.1 fusion.28
  145.3 0.2 fusion.12
  145.4 0.2 fusion.14
  145.6 1.0 concatenate.36
  146.6 5.7 %all-to-all-start.5 = ((f32[16,16,705]{2,1,0:T(8,128)}), f32[16,16,705]{2,1,0:T(8,128)S(1)}, u32[]{:S(2)}, u32[]{:S(2)}) async-start(f32[16,16,705]{2,1,0:T(8,128)} %concatenate.36), calls=%async_computation.5 | async-start | bytes 1572864 | tf_op jit(solution)/shard_map/all_to_all | solution.py:35
  152.5 22.6 %all-to-all-done.5 = f32[16,16,705]{2,1,0:T(8,128)S(1)} async-done(((f32[16,16,705]{2,1,0:T(8,128)}), f32[16,16,705]{2,1,0:T(8,128)S(1)}, u32[]{:S(2)}, u32[]{:S(2)}) %all-to-all-start.5) | async-done | bytes 721952 | tf_op jit(solution)/shard_map/all_to_all | solution.py:35
  175.1 0.2 fusion.89
  175.9 2.6 %fusion.2 = f32[16,4,64]{2,1,0:T(4,128)S(1)} fusion(f32[2,16,4,64,64]{4,3,2,1,0:T(8,128)} %param.34, f32[16,64]{1,0:T(8,128)S(1)} %divide_multiply_fusion.2, f32[16,64]{1,0:T(8,128)S(1)} %divide_multiply_fusion.3, f32[16,4,64]{2,1,0:T(4,128)S(1)} %fusion.44, f32[16,4]{1,0:T(8,128)S(1)} %get-tuple-element.7), kind=kLoop, calls=%fused_computation.4 | loop fusion | flops 1306624 | bytes 1089792 | tf_op jit(solution)/shard_map/reduce_sum | solution.py:60
  178.6 0.2 multiply_reduce_fusion.6
  178.9 0.7 broadcast_in_dim.57
  179.6 3.7 %all-to-all-start.6 = ((bf16[16,16,256]{2,1,0:T(8,128)(2,1)}), bf16[16,16,256]{2,1,0:T(8,128)(2,1)S(1)}, u32[]{:S(2)}, u32[]{:S(2)}) async-start(bf16[16,16,256]{2,1,0:T(8,128)(2,1)} %broadcast_in_dim.57), calls=%async_computation.6 | async-start | bytes 262144 | tf_op jit(solution)/shard_map/all_to_all | solution.py:21
  183.2 0.6 pad_maximum_fusion.4
  183.9 0.6 pad_maximum_fusion.5
  184.5 0.6 pad_maximum_fusion.1
  185.1 6.5 %all-to-all-done.6 = bf16[16,16,256]{2,1,0:T(8,128)(2,1)S(1)} async-done(((bf16[16,16,256]{2,1,0:T(8,128)(2,1)}), bf16[16,16,256]{2,1,0:T(8,128)(2,1)S(1)}, u32[]{:S(2)}, u32[]{:S(2)}) %all-to-all-start.6) | async-done | bytes 131104 | tf_op jit(solution)/shard_map/all_to_all | solution.py:21
  191.6 0.8 fusion.10
  192.4 4.0 %all-to-all-start.7 = ((f32[16,16,128]{2,1,0:T(8,128)}), f32[16,16,128]{2,1,0:T(8,128)S(1)}, u32[]{:S(2)}, u32[]{:S(2)}) async-start(f32[16,16,128]{2,1,0:T(8,128)} %fusion.10), calls=%async_computation.7 | async-start | bytes 262144 | tf_op jit(solution)/shard_map/all_to_all | solution.py:35
  196.4 3.7 %multiply_add_fusion.1 = (f32[1,16,4,64,64]{4,3,2,1,0:T(8,128)S(1)}, f32[1,16,4,64,64]{4,3,2,1,0:T(8,128)S(1)}) fusion(f32[2,16,4,64,64]{4,3,2,1,0:T(8,128)} %param.34, f32[16,64]{1,0:T(8,128)S(1)} %divide_multiply_fusion.5, f32[16,4,64]{2,1,0:T(4,128)S(1)} %fusion.45, f32[16,4]{1,0:T(8,128)S(1)} %get-tuple-element.11, ...), kind=kLoop, calls=%fused_computation.10 | loop fusion | flops 1572864 | bytes 4235776 | tf_op jit(solution)/shard_map/add | solution.py:58
  200.1 2.4 %pad_maximum_fusion = f32[2,16,4,64,64]{4,3,2,1,0:T(8,128)} fusion(f32[1,16,4,64,64]{4,3,2,1,0:T(8,128)S(1)} %get-tuple-element.14, f32[1,16,4,64,64]{4,3,2,1,0:T(8,128)S(1)} %get-tuple-element.13), kind=kLoop, calls=%fused_computation | loop fusion | flops 524288 | bytes 4194304 | tf_op jit(solution)/shard_map/stack | solution.py:168
  202.5 6.2 %all-to-all-done.7 = f32[16,16,128]{2,1,0:T(8,128)S(1)} async-done(((f32[16,16,128]{2,1,0:T(8,128)}), f32[16,16,128]{2,1,0:T(8,128)S(1)}, u32[]{:S(2)}, u32[]{:S(2)}) %all-to-all-start.7) | async-done | bytes 131104 | tf_op jit(solution)/shard_map/all_to_all | solution.py:35
  208.7 0.6 add_convert_fusion
  (76 shorter events, 1.9 us)
Async XLA Ops:
  2.0 55.6 %all-to-all-start = ((bf16[16,16,128]{2,1,0:T(8,128)(2,1)}), bf16[16,16,128]{2,1,0:T(8,128)(2,1)S(1)}, u32[]{:S(2)}, u32[]{:S(2)}) async-start(bf16[16,16,128]{2,1,0:T(8,128)(2,1)} %broadcast_in_dim.20), calls=%async_computation | async-start | bytes 131072 | tf_op jit(solution)/shard_map/all_to_all | solution.py:21
  60.4 12.7 %copy-start.13 = (f32[2,4]{1,0:T(2,128)S(1)}, f32[2,4]{1,0:T(2,128)}, u32[]{:S(2)}) copy-start(f32[2,4]{1,0:T(2,128)} %param.31) | copy-start | bytes 100
  60.4 12.9 %copy-start.11 = (bf16[2,4,64]{2,1,0:T(4,128)(2,1)S(1)}, bf16[2,4,64]{2,1,0:T(4,128)(2,1)}, u32[]{:S(2)}) copy-start(bf16[2,4,64]{2,1,0:T(4,128)(2,1)} %param.27) | copy-start | bytes 3076
  60.5 12.9 %copy-start.12 = (bf16[2,4,64]{2,1,0:T(4,128)(2,1)S(1)}, bf16[2,4,64]{2,1,0:T(4,128)(2,1)}, u32[]{:S(2)}) copy-start(bf16[2,4,64]{2,1,0:T(4,128)(2,1)} %param.28) | copy-start | bytes 3076
  60.5 12.9 %copy-start.10 = (bf16[2,4,256]{2,1,0:T(4,128)(2,1)S(1)}, bf16[2,4,256]{2,1,0:T(4,128)(2,1)}, u32[]{:S(2)}) copy-start(bf16[2,4,256]{2,1,0:T(4,128)(2,1)} %param.26) | copy-start | bytes 12292
  60.5 12.9 %copy-start.7 = (bf16[2,16,3,64]{3,1,2,0:T(8,128)(2,1)S(1)}, bf16[2,16,3,64]{3,1,2,0:T(8,128)(2,1)}, u32[]{:S(2)}) copy-start(bf16[2,16,3,64]{3,1,2,0:T(8,128)(2,1)} %param.36) | copy-start | bytes 36868
  60.5 12.9 %copy-start.8 = (bf16[2,16,3,64]{3,1,2,0:T(8,128)(2,1)S(1)}, bf16[2,16,3,64]{3,1,2,0:T(8,128)(2,1)}, u32[]{:S(2)}) copy-start(bf16[2,16,3,64]{3,1,2,0:T(8,128)(2,1)} %param.37) | copy-start | bytes 36868
  60.5 12.9 %copy-start.3 = (bf16[2,16,3,256]{3,1,2,0:T(8,128)(2,1)S(1)}, bf16[2,16,3,256]{3,1,2,0:T(8,128)(2,1)}, u32[]{:S(2)}) copy-start(bf16[2,16,3,256]{3,1,2,0:T(8,128)(2,1)} %param.35) | copy-start | bytes 147460
  63.6 32.3 %all-to-all-start.1 = ((f32[16,16,705]{2,1,0:T(8,128)}), f32[16,16,705]{2,1,0:T(8,128)S(1)}, u32[]{:S(2)}, u32[]{:S(2)}) async-start(f32[16,16,705]{2,1,0:T(8,128)} %concatenate.31), calls=%async_computation.1 | async-start | bytes 1572864 | tf_op jit(solution)/shard_map/all_to_all | solution.py:35
  73.3 38.2 %copy-start = (bf16[2,256,128]{2,1,0:T(8,128)(2,1)S(1)}, bf16[2,256,128]{2,1,0:T(8,128)(2,1)}, u32[]{:S(2)}) copy-start(bf16[2,256,128]{2,1,0:T(8,128)(2,1)} %param.33) | copy-start | bytes 393220
  95.9 31.2 %copy-start.9 = (bf16[16,128]{1,0:T(8,128)(2,1)S(1)}, bf16[16,128]{1,0:T(8,128)(2,1)}, u32[]{:S(2)}) copy-start(bf16[16,128]{1,0:T(8,128)(2,1)} %param.19) | copy-start | bytes 12292
  96.2 48.5 %copy-start.4 = (bf16[2,128,64]{1,2,0:T(8,128)(2,1)S(1)}, bf16[2,128,64]{1,2,0:T(8,128)(2,1)}, u32[]{:S(2)}) copy-start(bf16[2,128,64]{1,2,0:T(8,128)(2,1)} %param.23) | copy-start | bytes 98308
  96.5 48.4 %copy-start.5 = (bf16[2,128,64]{1,2,0:T(8,128)(2,1)S(1)}, bf16[2,128,64]{1,2,0:T(8,128)(2,1)}, u32[]{:S(2)}) copy-start(bf16[2,128,64]{1,2,0:T(8,128)(2,1)} %param.24) | copy-start | bytes 98308
  96.6 48.5 %copy-start.6 = (bf16[2,128,64]{1,2,0:T(8,128)(2,1)S(1)}, bf16[2,128,64]{1,2,0:T(8,128)(2,1)}, u32[]{:S(2)}) copy-start(bf16[2,128,64]{1,2,0:T(8,128)(2,1)} %param.25) | copy-start | bytes 98308
  96.6 48.6 %copy-start.1 = (bf16[2,128,256]{2,1,0:T(8,128)(2,1)S(1)}, bf16[2,128,256]{2,1,0:T(8,128)(2,1)}, u32[]{:S(2)}) copy-start(bf16[2,128,256]{2,1,0:T(8,128)(2,1)} %param.22) | copy-start | bytes 393220
  96.6 48.8 %copy-start.2 = (bf16[2,128,256]{2,1,0:T(8,128)(2,1)S(1)}, bf16[2,128,256]{2,1,0:T(8,128)(2,1)}, u32[]{:S(2)}) copy-start(bf16[2,128,256]{2,1,0:T(8,128)(2,1)} %param.21) | copy-start | bytes 393220
  146.6 28.5 %all-to-all-start.5 = ((f32[16,16,705]{2,1,0:T(8,128)}), f32[16,16,705]{2,1,0:T(8,128)S(1)}, u32[]{:S(2)}, u32[]{:S(2)}) async-start(f32[16,16,705]{2,1,0:T(8,128)} %concatenate.36), calls=%async_computation.5 | async-start | bytes 1572864 | tf_op jit(solution)/shard_map/all_to_all | solution.py:35
  179.6 12.1 %all-to-all-start.6 = ((bf16[16,16,256]{2,1,0:T(8,128)(2,1)}), bf16[16,16,256]{2,1,0:T(8,128)(2,1)S(1)}, u32[]{:S(2)}, u32[]{:S(2)}) async-start(bf16[16,16,256]{2,1,0:T(8,128)(2,1)} %broadcast_in_dim.57), calls=%async_computation.6 | async-start | bytes 262144 | tf_op jit(solution)/shard_map/all_to_all | solution.py:21
  192.4 16.3 %all-to-all-start.7 = ((f32[16,16,128]{2,1,0:T(8,128)}), f32[16,16,128]{2,1,0:T(8,128)S(1)}, u32[]{:S(2)}, u32[]{:S(2)}) async-start(f32[16,16,128]{2,1,0:T(8,128)} %fusion.10), calls=%async_computation.7 | async-start | bytes 262144 | tf_op jit(solution)/shard_map/all_to_all | solution.py:35
where the time goes:
time: 210 us; the launch traced here: 209 us
  starting transfers between devices  67.1 us (32%)
  waiting for transfers between devices  66.8 us (32%)
  blocking collectives  44.5 us (21%)
  other arithmetic  17.5 us (8%)
  matrix products  6.34 us (3%)
  local copies, waits for them, and re-layouts  5.93 us (3%)
    all_to_all x3, waiting for transfers between devices, summed_on_arrival(): lax.all_to_all(blocks, axis, split_axis=0, concat_axis=0, tiled=True)  51.2 us
    all_to_all x2, starting transfers between devices, copy_for_each(): return lax.all_to_all(copies, axis, split_axis=0, concat_axis=0, tiled=True)  47.9 us
    all_to_all x2, blocking collectives, copy_for_each(): return lax.all_to_all(copies, axis, split_axis=0, concat_axis=0, tiled=True)  29.2 us
    all_to_all x3, starting transfers between devices, summed_on_arrival(): lax.all_to_all(blocks, axis, split_axis=0, concat_axis=0, tiled=True)  19.2 us
    all_to_all x2, waiting for transfers between devices, copy_for_each(): return lax.all_to_all(copies, axis, split_axis=0, concat_axis=0, tiled=True)  15.6 us
    all_to_all x1, blocking collectives, summed_on_arrival(): lax.all_to_all(blocks, axis, split_axis=0, concat_axis=0, tiled=True)  15.4 us
    dot_general x10, matrix products, body(): jnp.dot(rows_piece, matrix, preferred_element_type=jnp.float32)  5.36 us
    reduce_sum x2, other arithmetic, mixer(): jnp.sum(state_next * c_state, axis=-1)  5.31 us
  transfers between devices with their start and end apart: 5, of which 5 were waited for; matrix products, arithmetic and copies ran while one was open for 5% of the time, Pallas kernels for 0%

commit v1 on v0

v1 whole, which is shorter than its diff:
```python
import functools

import jax
import jax.numpy as jnp
from jax import lax
from jax.experimental import pallas as pl
from jax.experimental.pallas import tpu as pltpu
from jax.sharding import PartitionSpec as P

EPSILON = 1e-05
F32 = jnp.float32
BF16 = jnp.bfloat16
MESH = pl.DeviceIdType.MESH
NT = (((1,), (1,)), ((), ()))
LANES = 128


def silu(v):
    return v * jax.nn.sigmoid(v)


def kernel(
    tp_n,
    dp_n,
    features,
    tok,
    gain,
    w_z,
    w_x,
    w_bt,
    w_ct,
    w_dtt,
    conv_x,
    conv_b,
    conv_c,
    dt_bias,
    a_log,
    d_skip,
    out_gain,
    w_out_h,
    ssm_h,
    s_x,
    s_b,
    s_c,
    res_o,
    ssm_oh,
    nx_o,
    nb_o,
    nc_o,
    a_buf,
    b_out,
    b_in,
    c_own,
    c_buf,
    d_out,
    d_in,
    r_buf,
    w_bcd,
    conv_bc,
    s_bc,
    st_t,
    w_out,
    ssm,
    ssm_o,
    local_sem,
    out_sem,
    send_sem,
    recv_sem,
):
    layers, heads_here = dt_bias.shape
    rows, width_f = tok.shape
    zw = w_z.shape[2]
    bw = w_bt.shape[1]
    hd = zw // heads_here
    my_tp, my_dp = lax.axis_index("tp"), lax.axis_index("dp")
    my_x, my_core = lax.div(my_dp, 2), lax.rem(my_dp, 2)
    dp_x = dp_n // 2

    def tp_at(k):
        off = jnp.where(lax.rem(k, 2) == 1, lax.div(k + 1, 2), tp_n - lax.div(k, 2))
        return lax.rem(my_tp + off, tp_n)

    def dp_at(k):
        m = lax.div(k, 2)
        off = jnp.where(lax.rem(m, 2) == 1, lax.div(m + 1, 2), dp_x - lax.div(m, 2))
        return lax.rem(my_x + off, dp_x) * 2 + lax.rem(my_core + k, 2)

    def remote(src, dst, layer, phase, s_slot, r_slot, axis, target):
        return pltpu.make_async_remote_copy(
            src_ref=src,
            dst_ref=dst,
            send_sem=send_sem.at[layer, phase, s_slot],
            recv_sem=recv_sem.at[layer, phase, r_slot],
            device_id={axis: target},
            device_id_type=MESH,
        )

    fetch = [
        pltpu.make_async_copy(ssm_h, ssm, local_sem.at[0]),
        pltpu.make_async_copy(w_out_h, w_out, local_sem.at[1]),
    ]
    for f in fetch:
        f.start()
    barrier = pltpu.get_barrier_semaphore()

    def greet_tp(k, carry):
        pl.semaphore_signal(barrier, inc=1, device_id={"tp": tp_at(k)}, device_id_type=MESH)
        return carry

    def greet_dp(k, carry):
        pl.semaphore_signal(barrier, inc=1, device_id={"dp": dp_at(k)}, device_id_type=MESH)
        return carry

    lax.fori_loop(1, tp_n, greet_tp, 0)
    lax.fori_loop(1, dp_n, greet_dp, 0)

    heads_all = w_dtt.shape[1]
    pick = lax.broadcasted_iota(jnp.int32, (16, heads_all), 0)
    col = lax.broadcasted_iota(jnp.int32, (16, heads_all), 1)
    pick = jnp.where((pick < heads_here) & (col == pick + my_tp * heads_here), 1.0, 0.0).astype(BF16)
    for l in range(layers):
        w_bcd[l, 0:bw] = w_bt[l]
        w_bcd[l, bw : 2 * bw] = w_ct[l]
        w_bcd[l, 2 * bw : 2 * bw + 16] = jnp.dot(
            pick, w_dtt[l], preferred_element_type=F32
        ).astype(BF16)
        w_bcd[l, 2 * bw + 16 :] = jnp.zeros((w_bcd.shape[1] - 2 * bw - 16, width_f), BF16)
        conv_bc[l] = jnp.concatenate([conv_b[l].astype(F32), conv_c[l].astype(F32)], axis=1)
        for k in range(s_b.shape[1]):
            s_bc[l, k] = jnp.concatenate([s_b[l, k].astype(F32), s_c[l, k].astype(F32)], axis=1)
    for f in fetch:
        f.wait()

    def turn(i, carry):
        for l in range(layers):
            block = ssm[l, i].reshape(zw, bw)
            st_t[l, i] = block.T.astype(BF16)
        return carry

    lax.fori_loop(0, rows, turn, 0)
    r_buf[0] = tok[...]
    pl.semaphore_wait(barrier, tp_n + dp_n - 2)

    lane = lax.broadcasted_iota(jnp.int32, (rows, LANES), 1)
    head_of = lax.broadcasted_iota(jnp.int32, (rows, zw), 1)
    head_of = lax.div(head_of, hd)

    def per_head(v):
        out = jnp.broadcast_to(v[:, 0:1], (rows, zw))
        for h in range(1, heads_here):
            out = jnp.where(head_of == h, v[:, h : h + 1], out)
        return out

    for l in range(layers):
        own_rows = r_buf.at[l]
        a_buf[l, my_tp] = r_buf[l]

        def send_a(n, carry, l=l, own_rows=own_rows):
            k = tp_n - 1 - n
            remote(own_rows, a_buf.at[l, my_tp], l, 0, k, my_tp, "tp", tp_at(k)).start()
            return carry

        lax.fori_loop(0, tp_n - 1, send_a, 0)

        def step_b(k, carry, l=l):
            i = tp_at(k)

            @pl.when(k > 0)
            def _():
                remote(a_buf.at[l, i], a_buf.at[l, i], l, 0, k, i, "tp", i).wait_recv()

            block = a_buf[l, i].astype(F32)
            scaled = (block * gain[l : l + 1].astype(F32)).astype(BF16)
            b_out[l, i, :, 0:zw] = jnp.dot(scaled, w_z[l], preferred_element_type=F32).astype(BF16)
            b_out[l, i, :, zw : 2 * zw] = jnp.dot(
                scaled, w_x[l], preferred_element_type=F32
            ).astype(BF16)
            rest = lax.dot_general(scaled, w_bcd[l], NT, preferred_element_type=F32)
            b_out[l, i, :, 2 * zw : 2 * zw + LANES] = rest[:, 0:LANES].astype(BF16)
            squares = jnp.sum(block * block, axis=1, keepdims=True)
            small = jnp.where(lane == heads_here, squares, rest[:, LANES:])
            low = small - small.astype(BF16).astype(F32)
            both = jnp.where(lane < LANES // 2, small, pltpu.roll(low, LANES // 2, 1))
            b_out[l, i, :, 2 * zw + LANES :] = both.astype(BF16)

            @pl.when(i != my_dp)
            def _():
                remote(b_out.at[l, i], b_in.at[l, my_dp], l, 1, i, my_dp, "dp", i).start()

            return carry

        lax.fori_loop(0, tp_n, step_b, 0)

        def add_b(k, total, l=l):
            i = dp_at(k)
            remote(b_in.at[l, i], b_in.at[l, i], l, 1, i, i, "dp", i).wait_recv()
            return total + b_in[l, i].astype(F32)

        total = lax.fori_loop(1, dp_n, add_b, b_out[l, my_dp].astype(F32))

        small = total[:, 2 * zw + LANES :]
        small = small + pltpu.roll(small, LANES // 2, 1)
        row_scale = lax.rsqrt(small[:, heads_here : heads_here + 1] / features + EPSILON)
        step_raw = small[:, 0:heads_here] * row_scale
        gate = (total[:, 0:zw] * row_scale).astype(BF16).astype(F32)
        x_new = (total[:, zw : 2 * zw] * row_scale).astype(BF16)
        bc_new = (total[:, 2 * zw : 2 * zw + LANES] * row_scale).astype(BF16)
        taps = conv_x.shape[1]
        conv = x_new.astype(F32) * conv_x[l, taps - 1 : taps].astype(F32)
        conv2 = bc_new.astype(F32) * conv_bc[l, taps - 1 : taps]
        for k in range(taps - 1):
            conv = conv + s_x[l, k].astype(F32) * conv_x[l, k : k + 1].astype(F32)
            conv2 = conv2 + s_bc[l, k] * conv_bc[l, k : k + 1]
        v = silu(conv)
        bc = silu(conv2)
        step = jax.nn.softplus(step_raw + dt_bias[l : l + 1])
        decay = jnp.exp(-step * jnp.exp(a_log[l : l + 1]))
        xs = per_head(step) * v
        turned = pltpu.roll(bc, LANES // 2, 1)
        b_dot_c = 0.5 * jnp.sum(bc * turned, axis=1, keepdims=True)
        cc = jnp.where(lane < LANES // 2, turned, bc)
        row = lax.broadcasted_iota(jnp.int32, (rows, LANES), 0)
        pieces = []
        for s in range(0, rows, 2):
            pieces.append(jnp.where(row == s + lax.div(lane, LANES // 2), cc, 0.0).astype(BF16))
        spread = jnp.concatenate(pieces, axis=1)
        reads = jnp.dot(
            spread, st_t[l].reshape(rows * bw, zw), preferred_element_type=F32
        )
        readout = per_head(decay) * reads + (xs * b_dot_c + per_head(d_skip[l : l + 1]) * v)
        gated = readout * silu(gate)
        scale = lax.rsqrt(jnp.mean(gated * gated, axis=1, keepdims=True) + EPSILON)
        mixed = (gated * scale * out_gain[l : l + 1].astype(F32)).astype(BF16)

        c_own[l] = mixed
        c_buf[l, my_dp] = mixed

        def send_c(n, carry, l=l):
            k = dp_n - 1 - n
            remote(c_own.at[l], c_buf.at[l, my_dp], l, 2, k, my_dp, "dp", dp_at(k)).start()
            return carry

        lax.fori_loop(0, dp_n - 1, send_c, 0)

        xs_t = xs.T
        for s in range(rows):
            for h in range(heads_here):
                b_row = bc[s : s + 1, 0:bw]
                column = xs_t[h * hd : (h + 1) * hd, s : s + 1]
                ssm_o[l, s, h] = ssm[l, s, h] * decay[s : s + 1, h : h + 1] + column * b_row
        pltpu.make_async_copy(ssm_o.at[l], ssm_oh.at[l], out_sem.at[l]).start()
        for k in range(taps - 2):
            nx_o[l, k] = s_x[l, k + 1]
            nb_o[l, k] = s_b[l, k + 1]
            nc_o[l, k] = s_c[l, k + 1]
        nx_o[l, taps - 2] = x_new
        nb_o[l, taps - 2] = bc_new[:, 0:bw]
        nc_o[l, taps - 2] = bc_new[:, bw : 2 * bw]

        def step_d(k, carry, l=l):
            i = dp_at(k)

            @pl.when(k > 0)
            def _():
                remote(c_buf.at[l, i], c_buf.at[l, i], l, 2, k, i, "dp", i).wait_recv()

            part = jnp.dot(c_buf[l, i], w_out[l], preferred_element_type=F32)
            d_out[l, i] = part.astype(BF16)

            @pl.when(i != my_tp)
            def _():
                remote(d_out.at[l, i], d_in.at[l, my_tp], l, 3, i, my_tp, "tp", i).start()

            return carry

        lax.fori_loop(0, dp_n, step_d, 0)

        def add_d(k, total, l=l):
            i = tp_at(k)
            remote(d_in.at[l, i], d_in.at[l, i], l, 3, i, i, "tp", i).wait_recv()
            return total + d_in[l, i].astype(F32)

        projected = lax.fori_loop(1, tp_n, add_d, d_out[l, my_tp].astype(F32))
        new = (r_buf[l].astype(F32) + projected).astype(BF16)
        if l + 1 < layers:
            r_buf[l + 1] = new
        else:
            res_o[...] = new

    for l in range(layers):

        def sent_tp(k, carry, l=l):
            i = tp_at(k)
            remote(r_buf.at[l], a_buf.at[l, my_tp], l, 0, k, my_tp, "tp", i).wait_send()
            remote(d_out.at[l, i], d_in.at[l, my_tp], l, 3, i, my_tp, "tp", i).wait_send()
            return carry

        def sent_dp(k, carry, l=l):
            i = dp_at(k)
            remote(b_out.at[l, i], b_in.at[l, my_dp], l, 1, i, my_dp, "dp", i).wait_send()
            remote(c_own.at[l], c_buf.at[l, my_dp], l, 2, k, my_dp, "dp", i).wait_send()
            return carry

        lax.fori_loop(1, tp_n, sent_tp, 0)
        lax.fori_loop(1, dp_n, sent_dp, 0)
        pltpu.make_async_copy(ssm_o.at[l], ssm_oh.at[l], out_sem.at[l]).wait()


def body(tp_n, dp_n, *args):
    (
        tokens,
        norm_gain,
        w_z,
        w_x,
        w_b,
        w_c,
        w_dt,
        conv_x,
        conv_b,
        conv_c,
        dt_bias,
        a_log,
        d_skip,
        out_gain,
        w_out,
        ssm_state,
        state_x,
        state_b,
        state_c,
    ) = args
    layers, heads_here = dt_bias.shape
    rows, width_f = tokens.shape
    zw, bw = w_z.shape[2], w_b.shape[2]
    assert tp_n == dp_n and 2 * bw == LANES
    wide = 2 * zw + 2 * LANES

    def turn(a):
        return jnp.swapaxes(a, 1, 2)

    operands = (
        tokens,
        norm_gain,
        w_z,
        w_x,
        turn(w_b),
        turn(w_c),
        turn(w_dt),
        conv_x,
        conv_b,
        conv_c,
        dt_bias,
        a_log,
        d_skip,
        out_gain,
        w_out,
        ssm_state,
        turn(state_x),
        turn(state_b),
        turn(state_c),
    )
    vmem = pl.BlockSpec(memory_space=pltpu.VMEM)
    hbm = pl.BlockSpec(memory_space=pl.ANY)
    in_specs = [vmem] * 14 + [hbm, hbm] + [vmem] * 3

    def like(a):
        return jax.ShapeDtypeStruct(a.shape, a.dtype)

    residual, ssm_next, next_x, next_b, next_c = pl.pallas_call(
        functools.partial(kernel, tp_n, dp_n, width_f * dp_n),
        out_shape=(
            like(tokens),
            like(ssm_state),
            like(operands[16]),
            like(operands[17]),
            like(operands[18]),
        ),
        in_specs=in_specs,
        out_specs=(vmem, hbm, vmem, vmem, vmem),
        scratch_shapes=[
            pltpu.VMEM((layers, tp_n, rows, width_f), BF16),
            pltpu.VMEM((layers, dp_n, rows, wide), BF16),
            pltpu.VMEM((layers, dp_n, rows, wide), BF16),
            pltpu.VMEM((layers, rows, zw), BF16),
            pltpu.VMEM((layers, dp_n, rows, zw), BF16),
            pltpu.VMEM((layers, tp_n, rows, width_f), BF16),
            pltpu.VMEM((layers, tp_n, rows, width_f), BF16),
            pltpu.VMEM((layers, rows, width_f), BF16),
            pltpu.VMEM((layers, 2 * LANES, width_f), BF16),
            pltpu.VMEM((layers, conv_x.shape[1], LANES), F32),
            pltpu.VMEM((layers, state_b.shape[2], rows, LANES), F32),
            pltpu.VMEM((layers, rows, bw, zw), BF16),
            pltpu.VMEM(w_out.shape, BF16),
            pltpu.VMEM(ssm_state.shape, F32),
            pltpu.VMEM(ssm_state.shape, F32),
            pltpu.SemaphoreType.DMA((2,)),
            pltpu.SemaphoreType.DMA((layers,)),
            pltpu.SemaphoreType.DMA((layers, 4, max(tp_n, dp_n))),
            pltpu.SemaphoreType.DMA((layers, 4, max(tp_n, dp_n))),
        ],
        compiler_params=pltpu.CompilerParams(collective_id=0, has_side_effects=True),
        name="decode",
    )(*operands)
    return residual, ssm_next, turn(next_x), turn(next_b), turn(next_c)


def solution(mesh):
    placed = (
        P(("grp", "tp"), "dp"),
        P(None, "dp"),
        P(None, "dp", "tp"),
        P(None, "dp", "tp"),
        P(None, "dp", "tp"),
        P(None, "dp", "tp"),
        P(None, "dp", None),
        P(None, None, "tp"),
        P(None, None, "tp"),
        P(None, None, "tp"),
        P(None, "tp"),
        P(None, "tp"),
        P(None, "tp"),
        P(None, "tp"),
        P(None, "tp", "dp"),
        P(None, ("grp", "dp"), "tp", None, None),
        P(None, ("grp", "dp"), None, "tp"),
        P(None, ("grp", "dp"), None, "tp"),
        P(None, ("grp", "dp"), None, "tp"),
    )
    return jax.shard_map(
        functools.partial(body, mesh.shape["tp"], mesh.shape["dp"]),
        mesh=mesh,
        in_specs=placed,
        out_specs=(placed[0], placed[15], placed[16], placed[17], placed[18]),
        check_vma=False,
    )
```

time: 210 us -> 123 us (0.59)
  Pallas kernels: 0 us -> 112 us
  starting transfers between devices: 67.1 us -> 0 us
  waiting for transfers between devices: 66.8 us -> 0 us
  blocking collectives: 44.5 us -> 0 us
  other arithmetic: 17.5 us -> 0 us
  matrix products: 6.34 us -> 0 us
    pallas_call x0 -> x1, Pallas kernels: none -> 112 us  [body(): pl.pallas_call(functools.partial(kernel, tp_n, dp_n, width_f * dp_n), out...]
    all_to_all x5 -> x0, starting transfers between devices: 67.1 us -> none  [the longest x2 47.9 us: copy_for_each(): return lax.all_to_all(copies, axis, split_axis=0, concat_axis=0, tiled=True)]
    all_to_all x5 -> x0, waiting for transfers between devices: 66.8 us -> none  [the longest x3 51.2 us: summed_on_arrival(): lax.all_to_all(blocks, axis, split_axis=0, concat_axis=0, tiled=True)]
    all_to_all x3 -> x0, blocking collectives: 44.5 us -> none  [the longest x2 29.2 us: copy_for_each(): return lax.all_to_all(copies, axis, split_axis=0, concat_axis=0, tiled=True)]
    unnamed x28 -> x11, local copies, waits for them, and re-layouts: 0.08 us -> 7.91 us
    dot_general x12 -> x0, matrix products: 6.34 us -> none  [the longest x10 5.36 us: body(): jnp.dot(rows_piece, matrix, preferred_element_type=jnp.float32)]
    reduce_sum x15 -> x0, other arithmetic: 6.11 us -> none  [the longest x2 5.31 us: mixer(): jnp.sum(state_next * c_state, axis=-1)]
    another operation x9 -> x0, other arithmetic: 4.34 us -> none  [the longest x1 2.45 us: body(): jnp.stack(states)]
  transfers between devices with their start and end apart: 5 -> 0, of which waited for: 5 -> 0; matrix products, arithmetic and copies ran while one was open for 5% -> 0% of each run, Pallas kernels for 0% -> 0%
where the time goes in v1:
time: 123 us; the launch traced here: 121 us
  Pallas kernels  112 us (91%)
  local copies, waits for them, and re-layouts  7.91 us (6%)
    pallas_call x1, Pallas kernels, body(): pl.pallas_call(functools.partial(kernel, tp_n, dp_n, width_f * dp_n), out...  112 us
    unnamed x11, local copies, waits for them, and re-layouts  7.91 us

profile of v1, /device:TPU:65, one launch (start us, length us, event | category | flops | bytes accessed | tf_op | source)
XLA Modules:
  0.0 120.9 jit_solution(537103601233417984)
XLA Ops:
  0.6 112.4 %decode.1 = (bf16[16,128]{1,0:T(8,128)(2,1)}, f32[2,16,4,64,64]{4,3,2,1,0:T(8,128)}, bf16[2,3,16,256]{3,2,1,0:T(8,128)(2,1)}, bf16[2,3,16,64]{3,2,1,0:T(8,128)(2,1)}, bf16[2,3,16,64]{3,2,1,0:T(8,128)(2,1)}) custom-call(bf16[16,128]{1,0:T(8,128)(2,1)} %tok.1, bf16[2,128]{1,0:T(2,128)(2,1)} %gain.1, bf16[2,128,256]{2,1,0:T(8,128)(2,1)} %w_z.1, ...), custom_call_target="tpu_custom_call" | custom-call | tf_op jit(solution)/shard_map/decode/pallas_call | solution.py:368
  113.0 1.3 %copy.29 = bf16[16,128]{1,0:T(8,128)(2,1)} copy(bf16[16,128]{1,0:T(8,128)(2,1)} %get-tuple-element.20) | data formatting | bytes 8192
  114.3 0.0 copy-start
  114.3 0.0 copy-start.2
  114.3 0.0 copy-start.1
  114.3 4.8 %copy.30 = f32[2,16,4,64,64]{4,3,2,1,0:T(8,128)} copy(f32[2,16,4,64,64]{4,3,2,1,0:T(8,128)} %get-tuple-element.21) | data formatting | bytes 4194304
  119.1 0.0 copy-done
  119.1 0.6 copy.31
  119.7 0.0 copy-done.2
  119.7 0.6 copy.32
  120.3 0.0 copy-done.1
  120.3 0.6 copy.33
Async XLA Ops:
  114.3 4.8 %copy-start = (bf16[2,3,16,256]{3,2,1,0:T(8,128)(2,1)S(1)}, bf16[2,3,16,256]{3,2,1,0:T(8,128)(2,1)}, u32[]{:S(2)}) copy-start(bf16[2,3,16,256]{3,2,1,0:T(8,128)(2,1)} %get-tuple-element.12) | copy-start | bytes 147460
  114.3 5.4 %copy-start.2 = (bf16[2,3,16,64]{3,2,1,0:T(8,128)(2,1)S(1)}, bf16[2,3,16,64]{3,2,1,0:T(8,128)(2,1)}, u32[]{:S(2)}) copy-start(bf16[2,3,16,64]{3,2,1,0:T(8,128)(2,1)} %get-tuple-element.13) | copy-start | bytes 36868
  114.3 6.0 %copy-start.1 = (bf16[2,3,16,64]{3,2,1,0:T(8,128)(2,1)S(1)}, bf16[2,3,16,64]{3,2,1,0:T(8,128)(2,1)}, u32[]{:S(2)}) copy-start(bf16[2,3,16,64]{3,2,1,0:T(8,128)(2,1)} %get-tuple-element.14) | copy-start | bytes 36868

commit v2 on v1

--- a/solution.py
+++ b/solution.py
@@ -13,6 +13,8 @@
 MESH = pl.DeviceIdType.MESH
 NT = (((1,), (1,)), ((), ()))
 LANES = 128
+INPUTS = 19
+GROUP = 4
 
 
 def silu(v):
@@ -23,52 +25,36 @@
     tp_n,
     dp_n,
     features,
-    tok,
-    gain,
-    w_z,
-    w_x,
-    w_bt,
-    w_ct,
-    w_dtt,
-    conv_x,
-    conv_b,
-    conv_c,
-    dt_bias,
-    a_log,
-    d_skip,
-    out_gain,
-    w_out_h,
-    ssm_h,
-    s_x,
-    s_b,
-    s_c,
-    res_o,
-    ssm_oh,
-    nx_o,
-    nb_o,
-    nc_o,
-    a_buf,
-    b_out,
-    b_in,
-    c_own,
-    c_buf,
-    d_out,
-    d_in,
-    r_buf,
-    w_bcd,
-    conv_bc,
-    s_bc,
-    st_t,
-    w_out,
-    ssm,
-    ssm_o,
-    local_sem,
-    out_sem,
-    send_sem,
-    recv_sem,
+    *refs,
 ):
+    held, refs = refs[:INPUTS], refs[INPUTS:]
+    res_o, ssm_o, nx_o, nb_o, nc_o = refs[:5]
+    a_buf, b_out, b_in, c_own, c_buf, d_out, d_in, r_buf = refs[5:13]
+    w_bcd, conv_bc, s_bc, st_t = refs[13:17]
+    here = refs[17 : 16 + INPUTS]
+    local_sem, send_sem, recv_sem = refs[16 + INPUTS :]
+    (
+        gain,
+        w_z,
+        w_x,
+        w_bt,
+        w_ct,
+        w_dtt,
+        conv_x,
+        conv_b,
+        conv_c,
+        dt_bias,
+        a_log,
+        d_skip,
+        out_gain,
+        w_out,
+        ssm,
+        s_x,
+        s_b,
+        s_c,
+    ) = here
     layers, heads_here = dt_bias.shape
-    rows, width_f = tok.shape
+    rows, width_f = res_o.shape
     zw = w_z.shape[2]
     bw = w_bt.shape[1]
     hd = zw // heads_here
@@ -84,6 +70,21 @@
         m = lax.div(k, 2)
         off = jnp.where(lax.rem(m, 2) == 1, lax.div(m + 1, 2), dp_x - lax.div(m, 2))
         return lax.rem(my_x + off, dp_x) * 2 + lax.rem(my_core + k, 2)
+
+    def mirror(k, n):
+        step = jnp.where(lax.rem(k, 2) == 1, k + 1, k - 1)
+        return jnp.where((k == n - 1) & (n % 2 == 0), k, jnp.where(k == 0, 0, step))
+
+    def nth(distance, n):
+        return jnp.where(distance <= n // 2, jnp.maximum(2 * distance - 1, 0), 2 * (n - distance))
+
+    def mirror_dp(k):
+        return 2 * mirror(lax.div(k, 2), dp_x) + lax.rem(k, 2)
+
+    k_rows = nth(lax.rem(my_dp - my_tp + tp_n, tp_n), tp_n)
+    k_sums = 2 * nth(lax.rem(lax.div(my_tp, 2) - my_x + dp_x, dp_x), dp_x) + lax.rem(
+        my_tp + my_core, 2
+    )
 
     def remote(src, dst, layer, phase, s_slot, r_slot, axis, target):
         return pltpu.make_async_remote_copy(
@@ -95,10 +96,9 @@
             device_id_type=MESH,
         )
 
-    fetch = [
-        pltpu.make_async_copy(ssm_h, ssm, local_sem.at[0]),
-        pltpu.make_async_copy(w_out_h, w_out, local_sem.at[1]),
-    ]
+    fetch = [pltpu.make_async_copy(held[0], r_buf.at[0], local_sem.at[0])]
+    for n in range(1, INPUTS):
+        fetch.append(pltpu.make_async_copy(held[n], here[n - 1], local_sem.at[n]))
     for f in fetch:
         f.start()
     barrier = pltpu.get_barrier_semaphore()
@@ -114,6 +114,8 @@
     lax.fori_loop(1, tp_n, greet_tp, 0)
     lax.fori_loop(1, dp_n, greet_dp, 0)
 
+    for f in fetch:
+        f.wait()
     heads_all = w_dtt.shape[1]
     pick = lax.broadcasted_iota(jnp.int32, (16, heads_all), 0)
     col = lax.broadcasted_iota(jnp.int32, (16, heads_all), 1)
@@ -128,8 +130,6 @@
         conv_bc[l] = jnp.concatenate([conv_b[l].astype(F32), conv_c[l].astype(F32)], axis=1)
         for k in range(s_b.shape[1]):
             s_bc[l, k] = jnp.concatenate([s_b[l, k].astype(F32), s_c[l, k].astype(F32)], axis=1)
-    for f in fetch:
-        f.wait()
 
     def turn(i, carry):
         for l in range(layers):
@@ -138,9 +138,9 @@
         return carry
 
     lax.fori_loop(0, rows, turn, 0)
-    r_buf[0] = tok[...]
     pl.semaphore_wait(barrier, tp_n + dp_n - 2)
 
+    lane_tall = lax.broadcasted_iota(jnp.int32, (GROUP * rows, LANES), 1)
     lane = lax.broadcasted_iota(jnp.int32, (rows, LANES), 1)
     head_of = lax.broadcasted_iota(jnp.int32, (rows, zw), 1)
     head_of = lax.div(head_of, hd)
@@ -152,51 +152,50 @@
         return out
 
     for l in range(layers):
-        own_rows = r_buf.at[l]
-        a_buf[l, my_tp] = r_buf[l]
-
-        def send_a(n, carry, l=l, own_rows=own_rows):
+        a_buf[l, 0] = r_buf[l]
+
+        def send_a(n, carry, l=l):
             k = tp_n - 1 - n
-            remote(own_rows, a_buf.at[l, my_tp], l, 0, k, my_tp, "tp", tp_at(k)).start()
+            slot = mirror(k, tp_n)
+            remote(r_buf.at[l], a_buf.at[l, slot], l, 0, k, slot, "tp", tp_at(k)).start()
             return carry
 
         lax.fori_loop(0, tp_n - 1, send_a, 0)
 
-        def step_b(k, carry, l=l):
-            i = tp_at(k)
-
-            @pl.when(k > 0)
-            def _():
-                remote(a_buf.at[l, i], a_buf.at[l, i], l, 0, k, i, "tp", i).wait_recv()
-
-            block = a_buf[l, i].astype(F32)
+        for first in range(0, tp_n, GROUP):
+            for k in range(max(first, 1), first + GROUP):
+                remote(a_buf.at[l, k], a_buf.at[l, k], l, 0, k, k, "tp", tp_at(k)).wait_recv()
+            tall = GROUP * rows
+            block = a_buf[l, first : first + GROUP].reshape(tall, width_f).astype(F32)
             scaled = (block * gain[l : l + 1].astype(F32)).astype(BF16)
-            b_out[l, i, :, 0:zw] = jnp.dot(scaled, w_z[l], preferred_element_type=F32).astype(BF16)
-            b_out[l, i, :, zw : 2 * zw] = jnp.dot(
-                scaled, w_x[l], preferred_element_type=F32
-            ).astype(BF16)
+            part_z = jnp.dot(scaled, w_z[l], preferred_element_type=F32).astype(BF16)
+            part_x = jnp.dot(scaled, w_x[l], preferred_element_type=F32).astype(BF16)
             rest = lax.dot_general(scaled, w_bcd[l], NT, preferred_element_type=F32)
-            b_out[l, i, :, 2 * zw : 2 * zw + LANES] = rest[:, 0:LANES].astype(BF16)
             squares = jnp.sum(block * block, axis=1, keepdims=True)
-            small = jnp.where(lane == heads_here, squares, rest[:, LANES:])
+            small = jnp.where(lane_tall == heads_here, squares, rest[:, LANES:])
             low = small - small.astype(BF16).astype(F32)
-            both = jnp.where(lane < LANES // 2, small, pltpu.roll(low, LANES // 2, 1))
-            b_out[l, i, :, 2 * zw + LANES :] = both.astype(BF16)
-
-            @pl.when(i != my_dp)
-            def _():
-                remote(b_out.at[l, i], b_in.at[l, my_dp], l, 1, i, my_dp, "dp", i).start()
-
-            return carry
-
-        lax.fori_loop(0, tp_n, step_b, 0)
+            both = jnp.where(lane_tall < LANES // 2, small, pltpu.roll(low, LANES // 2, 1))
+            b_out[l, first : first + GROUP, :, 0:zw] = part_z.reshape(GROUP, rows, zw)
+            b_out[l, first : first + GROUP, :, zw : 2 * zw] = part_x.reshape(GROUP, rows, zw)
+            b_out[l, first : first + GROUP, :, 2 * zw : 2 * zw + LANES] = (
+                rest[:, 0:LANES].astype(BF16).reshape(GROUP, rows, LANES)
+            )
+            b_out[l, first : first + GROUP, :, 2 * zw + LANES :] = both.astype(BF16).reshape(
+                GROUP, rows, LANES
+            )
+            for k in range(first, first + GROUP):
+                i = tp_at(k)
+
+                @pl.when(i != my_dp)
+                def _(k=k, i=i):
+                    remote(b_out.at[l, k], b_in.at[l, my_dp], l, 1, k, my_dp, "dp", i).start()
 
         def add_b(k, total, l=l):
             i = dp_at(k)
-            remote(b_in.at[l, i], b_in.at[l, i], l, 1, i, i, "dp", i).wait_recv()
+            remote(b_in.at[l, i], b_in.at[l, i], l, 1, k, i, "dp", i).wait_recv()
             return total + b_in[l, i].astype(F32)
 
-        total = lax.fori_loop(1, dp_n, add_b, b_out[l, my_dp].astype(F32))
+        total = lax.fori_loop(1, dp_n, add_b, b_out[l, k_rows].astype(F32))
 
         small = total[:, 2 * zw + LANES :]
         small = small + pltpu.roll(small, LANES // 2, 1)
@@ -233,14 +232,28 @@
         mixed = (gated * scale * out_gain[l : l + 1].astype(F32)).astype(BF16)
 
         c_own[l] = mixed
-        c_buf[l, my_dp] = mixed
+        c_buf[l, 0] = mixed
 
         def send_c(n, carry, l=l):
             k = dp_n - 1 - n
-            remote(c_own.at[l], c_buf.at[l, my_dp], l, 2, k, my_dp, "dp", dp_at(k)).start()
+            slot = mirror_dp(k)
+            remote(c_own.at[l], c_buf.at[l, slot], l, 2, k, slot, "dp", dp_at(k)).start()
             return carry
 
         lax.fori_loop(0, dp_n - 1, send_c, 0)
+
+        for first in range(0, dp_n, GROUP):
+            for k in range(max(first, 1), first + GROUP):
+                remote(c_buf.at[l, k], c_buf.at[l, k], l, 2, k, k, "dp", dp_at(k)).wait_recv()
+            block = c_buf[l, first : first + GROUP].reshape(GROUP * rows, zw)
+            part = jnp.dot(block, w_out[l], preferred_element_type=F32).astype(BF16)
+            d_out[l, first : first + GROUP] = part.reshape(GROUP, rows, width_f)
+            for k in range(first, first + GROUP):
+                i = dp_at(k)
+
+                @pl.when(i != my_tp)
+                def _(k=k, i=i):
+                    remote(d_out.at[l, k], d_in.at[l, my_tp], l, 3, k, my_tp, "tp", i).start()
 
         xs_t = xs.T
         for s in range(rows):
@@ -248,7 +261,6 @@
                 b_row = bc[s : s + 1, 0:bw]
                 column = xs_t[h * hd : (h + 1) * hd, s : s + 1]
                 ssm_o[l, s, h] = ssm[l, s, h] * decay[s : s + 1, h : h + 1] + column * b_row
-        pltpu.make_async_copy(ssm_o.at[l], ssm_oh.at[l], out_sem.at[l]).start()
         for k in range(taps - 2):
             nx_o[l, k] = s_x[l, k + 1]
             nb_o[l, k] = s_b[l, k + 1]
@@ -257,30 +269,12 @@
         nb_o[l, taps - 2] = bc_new[:, 0:bw]
         nc_o[l, taps - 2] = bc_new[:, bw : 2 * bw]
 
-        def step_d(k, carry, l=l):
-            i = dp_at(k)
-
-            @pl.when(k > 0)
-            def _():
-                remote(c_buf.at[l, i], c_buf.at[l, i], l, 2, k, i, "dp", i).wait_recv()
-
-            part = jnp.dot(c_buf[l, i], w_out[l], preferred_element_type=F32)
-            d_out[l, i] = part.astype(BF16)
-
-            @pl.when(i != my_tp)
-            def _():
-                remote(d_out.at[l, i], d_in.at[l, my_tp], l, 3, i, my_tp, "tp", i).start()
-
-            return carry
-
-        lax.fori_loop(0, dp_n, step_d, 0)
-
         def add_d(k, total, l=l):
             i = tp_at(k)
-            remote(d_in.at[l, i], d_in.at[l, i], l, 3, i, i, "tp", i).wait_recv()
+            remote(d_in.at[l, i], d_in.at[l, i], l, 3, k, i, "tp", i).wait_recv()
             return total + d_in[l, i].astype(F32)
 
-        projected = lax.fori_loop(1, tp_n, add_d, d_out[l, my_tp].astype(F32))
+        projected = lax.fori_loop(1, tp_n, add_d, d_out[l, k_sums].astype(F32))
         new = (r_buf[l].astype(F32) + projected).astype(BF16)
         if l + 1 < layers:
             r_buf[l + 1] = new
@@ -289,21 +283,39 @@
 
     for l in range(layers):
 
-        def sent_tp(k, carry, l=l):
-            i = tp_at(k)
-            remote(r_buf.at[l], a_buf.at[l, my_tp], l, 0, k, my_tp, "tp", i).wait_send()
-            remote(d_out.at[l, i], d_in.at[l, my_tp], l, 3, i, my_tp, "tp", i).wait_send()
+        def sent(k, carry, l=l):
+            i, j = tp_at(k), dp_at(k)
+            remote(r_buf.at[l], a_buf.at[l, 0], l, 0, k, 0, "tp", i).wait_send()
+            remote(c_own.at[l], c_buf.at[l, 0], l, 2, k, 0, "dp", j).wait_send()
             return carry
 
-        def sent_dp(k, carry, l=l):
-            i = dp_at(k)
-            remote(b_out.at[l, i], b_in.at[l, my_dp], l, 1, i, my_dp, "dp", i).wait_send()
-            remote(c_own.at[l], c_buf.at[l, my_dp], l, 2, k, my_dp, "dp", i).wait_send()
+        def sent_parts(k, carry, l=l):
+            i, j = tp_at(k), dp_at(k)
+
+            @pl.when(i != my_dp)
+            def _():
+                remote(b_out.at[l, k], b_in.at[l, my_dp], l, 1, k, my_dp, "dp", i).wait_send()
+
+            @pl.when(j != my_tp)
+            def _():
+                remote(d_out.at[l, k], d_in.at[l, my_tp], l, 3, k, my_tp, "tp", j).wait_send()
+
             return carry
 
-        lax.fori_loop(1, tp_n, sent_tp, 0)
-        lax.fori_loop(1, dp_n, sent_dp, 0)
-        pltpu.make_async_copy(ssm_o.at[l], ssm_oh.at[l], out_sem.at[l]).wait()
+        lax.fori_loop(1, tp_n, sent, 0)
+        lax.fori_loop(0, tp_n, sent_parts, 0)
+
+
+def write_out(*refs):
+    sem = refs[-1]
+    half = len(refs) // 2
+    copies = [
+        pltpu.make_async_copy(refs[n], refs[half + n], sem.at[n]) for n in range(half)
+    ]
+    for c in copies:
+        c.start()
+    for c in copies:
+        c.wait()
 
 
 def body(tp_n, dp_n, *args):
@@ -359,13 +371,12 @@
         turn(state_c),
     )
     vmem = pl.BlockSpec(memory_space=pltpu.VMEM)
-    hbm = pl.BlockSpec(memory_space=pl.ANY)
-    in_specs = [vmem] * 14 + [hbm, hbm] + [vmem] * 3
+    hbm = pl.BlockSpec(memory_space=pltpu.HBM)
 
     def like(a):
-        return jax.ShapeDtypeStruct(a.shape, a.dtype)
-
-    residual, ssm_next, next_x, next_b, next_c = pl.pallas_call(
+        return pltpu.VMEM(a.shape, a.dtype)
+
+    results = pl.pallas_call(
         functools.partial(kernel, tp_n, dp_n, width_f * dp_n),
         out_shape=(
             like(tokens),
@@ -374,8 +385,8 @@
             like(operands[17]),
             like(operands[18]),
         ),
-        in_specs=in_specs,
-        out_specs=(vmem, hbm, vmem, vmem, vmem),
+        in_specs=[hbm] * INPUTS,
+        out_specs=(vmem,) * 5,
         scratch_shapes=[
             pltpu.VMEM((layers, tp_n, rows, width_f), BF16),
             pltpu.VMEM((layers, dp_n, rows, wide), BF16),
@@ -389,17 +400,26 @@
             pltpu.VMEM((layers, conv_x.shape[1], LANES), F32),
             pltpu.VMEM((layers, state_b.shape[2], rows, LANES), F32),
             pltpu.VMEM((layers, rows, bw, zw), BF16),
-            pltpu.VMEM(w_out.shape, BF16),
-            pltpu.VMEM(ssm_state.shape, F32),
-            pltpu.VMEM(ssm_state.shape, F32),
-            pltpu.SemaphoreType.DMA((2,)),
-            pltpu.SemaphoreType.DMA((layers,)),
+            *(pltpu.VMEM(a.shape, a.dtype) for a in operands[1:]),
+            pltpu.SemaphoreType.DMA((INPUTS,)),
             pltpu.SemaphoreType.DMA((layers, 4, max(tp_n, dp_n))),
             pltpu.SemaphoreType.DMA((layers, 4, max(tp_n, dp_n))),
         ],
-        compiler_params=pltpu.CompilerParams(collective_id=0, has_side_effects=True),
+        compiler_params=pltpu.CompilerParams(
+            collective_id=0, has_side_effects=True, vmem_limit_bytes=40 * 1024 * 1024
+        ),
         name="decode",
-    )(*operands)
+    )(*(pltpu.with_memory_space_constraint(a, pltpu.HBM) for a in operands))
+    results = [pltpu.with_memory_space_constraint(a, pltpu.VMEM) for a in results]
+    residual, ssm_next, next_x, next_b, next_c = pl.pallas_call(
+        write_out,
+        out_shape=tuple(jax.ShapeDtypeStruct(a.shape, a.dtype) for a in results),
+        in_specs=(vmem,) * 5,
+        out_specs=(hbm,) * 5,
+        scratch_shapes=[pltpu.SemaphoreType.DMA((5,))],
+        compiler_params=pltpu.CompilerParams(vmem_limit_bytes=8 * 1024 * 1024),
+        name="write_out",
+    )(*results)
     return residual, ssm_next, turn(next_x), turn(next_b), turn(next_c)
 
 

time: 123 us -> 117 us (0.951); the launches traced: 121 us -> 117 us
  local copies, waits for them, and re-layouts: 7.91 us -> 0 us
  Pallas kernels: 112 us -> 116 us
    unnamed x11 -> x0, local copies, waits for them, and re-layouts: 7.91 us -> none
    pallas_call x0 -> x1, Pallas kernels: none -> 2.07 us  [body(): pl.pallas_call(write_out, out_shape=tuple((jax.ShapeDtypeStruct(a.shape,...]
    pallas_call x1, Pallas kernels: 112 us -> 114 us  [body(): pl.pallas_call(functools.partial(kernel, tp_n, dp_n, width_f * dp_n), out...]
where the time goes in v2:
time: 117 us
  Pallas kernels  116 us (99%)
    pallas_call x1, Pallas kernels, body(): pl.pallas_call(functools.partial(kernel, tp_n, dp_n, width_f * dp_n), out...  114 us

profile of v2, /device:TPU:65, one launch (start us, length us, event | category | flops | bytes accessed | tf_op | source)
XLA Modules:
  0.0 117.0 jit_solution(10615264600704511785)
XLA Ops:
  0.6 114.3 %decode.1 = (bf16[16,128]{1,0:T(8,128)(2,1)S(1)}, f32[2,16,4,64,64]{4,3,2,1,0:T(8,128)S(1)}, bf16[2,3,16,256]{3,2,1,0:T(8,128)(2,1)S(1)}, bf16[2,3,16,64]{3,2,1,0:T(8,128)(2,1)S(1)}, bf16[2,3,16,64]{3,2,1,0:T(8,128)(2,1)S(1)}) custom-call(bf16[16,128]{1,0:T(8,128)(2,1)} %refs_0_.1, bf16[2,128]{1,0:T(2,128)(2,1)} %refs_1_.1, bf16[2,128,256]{2,1,0:T(8,128)(2,1)} %refs_2_.1, ...), custom_call_target="tpu_custom_call" | custom-call | tf_op jit(solution)/shard_map/decode/pallas_call | solution.py:379
  114.9 2.1 %write_out.1 = (bf16[16,128]{1,0:T(8,128)(2,1)}, f32[2,16,4,64,64]{4,3,2,1,0:T(8,128)}, bf16[2,3,16,256]{3,2,1,0:T(8,128)(2,1)}, bf16[2,3,16,64]{3,2,1,0:T(8,128)(2,1)}, bf16[2,3,16,64]{3,2,1,0:T(8,128)(2,1)}) custom-call(bf16[16,128]{1,0:T(8,128)(2,1)S(1)} %get-tuple-element.15.refs_0_, f32[2,16,4,64,64]{4,3,2,1,0:T(8,128)S(1)} %get-tuple-element.16.refs_1_, ...), custom_call_target="tpu_custom_call" | custom-call | tf_op jit(solution)/shard_map/write_out/pallas_call | solution.py:414

commit v3 on v2

v3 whole, which is shorter than its diff:
```python
import functools

import jax
import jax.numpy as jnp
from jax import lax
from jax.experimental import pallas as pl
from jax.experimental.pallas import tpu as pltpu
from jax.sharding import PartitionSpec as P

EPSILON = 1e-05
F32 = jnp.float32
BF16 = jnp.bfloat16
MESH = pl.DeviceIdType.MESH
NT = (((1,), (1,)), ((), ()))
LANES = 128
INPUTS = 19
GROUP = 4


def silu(v):
    return v * jax.nn.sigmoid(v)


def kernel(
    tp_n,
    dp_n,
    features,
    *refs,
):
    held, refs = refs[:INPUTS], refs[INPUTS:]
    res_o, ssm_o, nx_o, nb_o, nc_o = refs[:5]
    a_buf, b_out, b_in, c_own, c_buf, d_out, d_in, r_buf = refs[5:13]
    w_z, w_x, w_out, w_bcd, gains, conv_bc, s_bc, st_t = refs[13:21]
    here = refs[21 : 17 + INPUTS]
    local_sem, pair_sem, send_sem, recv_sem = refs[17 + INPUTS :]
    (
        gain,
        w_bt,
        w_ct,
        w_dtt,
        conv_x,
        conv_b,
        conv_c,
        dt_bias,
        a_log,
        d_skip,
        out_gain,
        ssm,
        s_x,
        s_b,
        s_c,
    ) = here
    layers, heads_here = dt_bias.shape
    rows, width_f = res_o.shape
    zw = w_z.shape[3]
    bw = w_bt.shape[1]
    hd = zw // heads_here
    my_tp, my_dp = lax.axis_index("tp"), lax.axis_index("dp")
    my_x, my_core = lax.div(my_dp, 2), lax.rem(my_dp, 2)
    half = tp_n // 2
    uneven = lax.rem(my_tp + my_core, 2) == 1
    row_core = lax.rem(my_tp, 2)

    def nearest(k, n):
        return jnp.where(lax.rem(k, 2) == 1, lax.div(k + 1, 2), lax.rem(n - lax.div(k, 2), n))

    def place(distance, n):
        return jnp.where(distance <= n // 2, jnp.maximum(2 * distance - 1, 0), 2 * (n - distance))

    def tp_at(k):
        return lax.rem(my_tp + nearest(k, tp_n), tp_n)

    def x_at(k):
        return lax.rem(my_x + nearest(k, half), half)

    def rows_at(k):
        odd = jnp.where(lax.rem(k, 2) == 0, k + 1, tp_n - k)
        return lax.rem(my_tp + jnp.where(uneven, odd, 2 * nearest(k, half)), tp_n)

    def rows_place(offset):
        odd = jnp.where(offset < half, offset - 1, tp_n - offset)
        return jnp.where(lax.rem(offset, 2) == 1, odd, place(lax.div(offset, 2), half))

    def x_mirror(k):
        step = jnp.where(lax.rem(k, 2) == 1, k + 1, k - 1)
        return jnp.where((k == half - 1) & (half % 2 == 0), k, jnp.where(k == 0, 0, step))

    k_rows = rows_place(lax.rem(my_dp - my_tp + tp_n, tp_n))

    def remote(src, dst, layer, phase, s_slot, r_slot, target):
        return pltpu.make_async_remote_copy(
            src_ref=src,
            dst_ref=dst,
            send_sem=send_sem.at[layer, phase, s_slot],
            recv_sem=recv_sem.at[layer, phase, r_slot],
            device_id=target,
            device_id_type=MESH,
        )

    def column(z, core):
        return {"tp": z, "dp": 2 * my_x + core}

    def row(x):
        return {"dp": 2 * x + my_core}

    layer_list = range(layers)
    fetch = [pltpu.make_async_copy(held[0], r_buf.at[0], local_sem.at[0])]
    used = 1
    for n in range(3):
        whole = (w_z, w_x, w_out)[n]
        for l in layer_list:
            fetch.append(
                pltpu.make_async_copy(
                    held[1 + n].at[l], whole.at[l, my_core], local_sem.at[used]
                )
            )
            used += 1
    for n in range(4, INPUTS):
        fetch.append(pltpu.make_async_copy(held[n], here[n - 4], local_sem.at[used]))
        used += 1
    for f in fetch:
        f.start()
    barrier = pltpu.get_barrier_semaphore()

    def greet(device):
        pl.semaphore_signal(barrier, inc=1, device_id=device, device_id_type=MESH)

    def greet_tp(k, carry):
        greet(column(tp_at(k), 0))
        greet(column(tp_at(k), 1))
        return carry

    def greet_dp(k, carry):
        greet(row(x_at(k)))
        return carry

    greet(column(my_tp, 1 - my_core))
    lax.fori_loop(1, tp_n, greet_tp, 0)
    lax.fori_loop(1, half, greet_dp, 0)

    for f in fetch:
        f.wait()
    heads_all = w_dtt.shape[1]
    pick = lax.broadcasted_iota(jnp.int32, (16, heads_all), 0)
    col = lax.broadcasted_iota(jnp.int32, (16, heads_all), 1)
    pick = jnp.where((pick < heads_here) & (col == pick + my_tp * heads_here), 1.0, 0.0).astype(BF16)
    for l in range(layers):
        w_bcd[l, my_core, 0:bw] = w_bt[l]
        w_bcd[l, my_core, bw : 2 * bw] = w_ct[l]
        w_bcd[l, my_core, 2 * bw : 2 * bw + 16] = jnp.dot(
            pick, w_dtt[l], preferred_element_type=F32
        ).astype(BF16)
        w_bcd[l, my_core, 2 * bw + 16 :] = jnp.zeros(
            (w_bcd.shape[2] - 2 * bw - 16, width_f), BF16
        )
        conv_bc[l] = jnp.concatenate([conv_b[l].astype(F32), conv_c[l].astype(F32)], axis=1)
        for k in range(s_b.shape[1]):
            s_bc[l, k] = jnp.concatenate([s_b[l, k].astype(F32), s_c[l, k].astype(F32)], axis=1)

    gains[my_core] = jnp.zeros(gains.shape[1:], F32)
    gains[my_core, 0:layers] = gain[...].astype(F32)

    def turn(i, carry):
        for l in range(layers):
            block = ssm[l, i].reshape(zw, bw)
            st_t[l, i] = block.T.astype(BF16)
        return carry

    lax.fori_loop(0, rows, turn, 0)
    pl.semaphore_wait(barrier, 2 * tp_n - 1 + half - 1)

    pair = []
    for whole in [gains.at[my_core]] + [
        w.at[l, my_core] for l in layer_list for w in (w_z, w_x, w_bcd, w_out)
    ]:
        pair.append(
            pltpu.make_async_remote_copy(
                src_ref=whole,
                dst_ref=whole,
                send_sem=pair_sem.at[0, len(pair)],
                recv_sem=pair_sem.at[1, len(pair)],
                device_id=column(my_tp, 1 - my_core),
                device_id_type=MESH,
            )
        )

    lane = lax.broadcasted_iota(jnp.int32, (rows, LANES), 1)
    head_of = lax.broadcasted_iota(jnp.int32, (rows, zw), 1)
    head_of = lax.div(head_of, hd)

    def per_head(v):
        out = jnp.broadcast_to(v[:, 0:1], (rows, zw))
        for h in range(1, heads_here):
            out = jnp.where(head_of == h, v[:, h : h + 1], out)
        return out

    for l in range(layers):
        def send_a(n, carry, l=l):
            k = tp_n - 1 - n
            z = tp_at(k)
            slot = 2 * rows_place(lax.rem(my_tp - z + tp_n, tp_n)) + my_core
            dst = a_buf.at[l, lax.div(slot, 2), my_core]
            remote(r_buf.at[l], dst, l, 0, k, slot, column(z, row_core)).start()
            return carry

        lax.fori_loop(0, tp_n - 1, send_a, 0)

        @pl.when(uneven)
        def _(l=l):
            dst = a_buf.at[l, 0, my_core]
            remote(r_buf.at[l], dst, l, 0, 0, my_core, column(my_tp, row_core)).start()

        @pl.when(jnp.logical_not(uneven))
        def _(l=l):
            a_buf[l, 0, my_core] = r_buf[l]

        if l == 0:
            for p in pair:
                p.start()

        for first in range(0, half, GROUP):
            group = min(GROUP, half)
            for k in range(first, first + group):
                for core in range(2):
                    got = a_buf.at[l, k, core]
                    copy = remote(got, got, l, 0, k, 2 * k + core, column(rows_at(k), core))
                    if k > 0:
                        copy.wait_recv()
                    else:

                        @pl.when(uneven | (my_core != core))
                        def _(copy=copy):
                            copy.wait_recv()

            if l == 0 and first == 0:
                for p in pair:
                    p.wait_recv()
            tall = group * rows
            scaled, squares = [], 0.0
            for core in range(2):
                block = a_buf[l, first : first + group, core].reshape(tall, width_f).astype(F32)
                scaled.append((block * gains[core, l : l + 1]).astype(BF16))
                squares = squares + jnp.sum(block * block, axis=1, keepdims=True)
            both_wide = jnp.concatenate(scaled, axis=1)
            part_z = jnp.dot(
                both_wide, w_z[l].reshape(2 * width_f, zw), preferred_element_type=F32
            ).astype(BF16)
            part_x = jnp.dot(
                both_wide, w_x[l].reshape(2 * width_f, zw), preferred_element_type=F32
            ).astype(BF16)
            rest = lax.dot_general(scaled[0], w_bcd[l, 0], NT, preferred_element_type=F32)
            rest += lax.dot_general(scaled[1], w_bcd[l, 1], NT, preferred_element_type=F32)
            lane_tall = lax.broadcasted_iota(jnp.int32, (tall, LANES), 1)
            small = jnp.where(lane_tall == heads_here, squares, rest[:, LANES:])
            low = small - small.astype(BF16).astype(F32)
            both = jnp.where(lane_tall < LANES // 2, small, pltpu.roll(low, LANES // 2, 1))
            b_out[l, first : first + group, :, 0:zw] = part_z.reshape(group, rows, zw)
            b_out[l, first : first + group, :, zw : 2 * zw] = part_x.reshape(group, rows, zw)
            b_out[l, first : first + group, :, 2 * zw : 2 * zw + LANES] = (
                rest[:, 0:LANES].astype(BF16).reshape(group, rows, LANES)
            )
            b_out[l, first : first + group, :, 2 * zw + LANES :] = both.astype(BF16).reshape(
                group, rows, LANES
            )
            for k in range(first, first + group):
                i = rows_at(k)

                @pl.when(i != my_dp)
                def _(k=k, i=i):
                    dst = b_in.at[l, my_x]
                    remote(b_out.at[l, k], dst, l, 1, k, my_x, row(lax.div(i, 2))).start()

        def add_b(k, total, l=l):
            x = x_at(k)
            remote(b_in.at[l, x], b_in.at[l, x], l, 1, k, x, row(x)).wait_recv()
            return total + b_in[l, x].astype(F32)

        total = lax.fori_loop(1, half, add_b, b_out[l, k_rows].astype(F32))

        small = total[:, 2 * zw + LANES :]
        small = small + pltpu.roll(small, LANES // 2, 1)
        row_scale = lax.rsqrt(small[:, heads_here : heads_here + 1] / features + EPSILON)
        step_raw = small[:, 0:heads_here] * row_scale
        gate = (total[:, 0:zw] * row_scale).astype(BF16).astype(F32)
        x_new = (total[:, zw : 2 * zw] * row_scale).astype(BF16)
        bc_new = (total[:, 2 * zw : 2 * zw + LANES] * row_scale).astype(BF16)
        taps = conv_x.shape[1]
        conv = x_new.astype(F32) * conv_x[l, taps - 1 : taps].astype(F32)
        conv2 = bc_new.astype(F32) * conv_bc[l, taps - 1 : taps]
        for k in range(taps - 1):
            conv = conv + s_x[l, k].astype(F32) * conv_x[l, k : k + 1].astype(F32)
            conv2 = conv2 + s_bc[l, k] * conv_bc[l, k : k + 1]
        v = silu(conv)
        bc = silu(conv2)
        step = jax.nn.softplus(step_raw + dt_bias[l : l + 1])
        decay = jnp.exp(-step * jnp.exp(a_log[l : l + 1]))
        xs = per_head(step) * v
        turned = pltpu.roll(bc, LANES // 2, 1)
        b_dot_c = 0.5 * jnp.sum(bc * turned, axis=1, keepdims=True)
        cc = jnp.where(lane < LANES // 2, turned, bc)
        seq = lax.broadcasted_iota(jnp.int32, (rows, LANES), 0)
        pieces = []
        for s in range(0, rows, 2):
            pieces.append(jnp.where(seq == s + lax.div(lane, LANES // 2), cc, 0.0).astype(BF16))
        spread = jnp.concatenate(pieces, axis=1)
        reads = jnp.dot(
            spread, st_t[l].reshape(rows * bw, zw), preferred_element_type=F32
        )
        readout = per_head(decay) * reads + (xs * b_dot_c + per_head(d_skip[l : l + 1]) * v)
        gated = readout * silu(gate)
        scale = lax.rsqrt(jnp.mean(gated * gated, axis=1, keepdims=True) + EPSILON)
        mixed = (gated * scale * out_gain[l : l + 1].astype(F32)).astype(BF16)

        c_own[l] = mixed
        c_buf[l, 0] = mixed

        def send_c(n, carry, l=l):
            k = half - 1 - n
            slot = x_mirror(k)
            remote(c_own.at[l], c_buf.at[l, slot], l, 2, k, slot, row(x_at(k))).start()
            return carry

        lax.fori_loop(0, half - 1, send_c, 0)

        for first in range(0, half, GROUP):
            group = min(GROUP, half)
            for k in range(max(first, 1), first + group):
                got = c_buf.at[l, k]
                remote(got, got, l, 2, k, k, row(x_at(k))).wait_recv()
            block = c_buf[l, first : first + group].reshape(group * rows, zw)
            for core in range(2):
                part = jnp.dot(block, w_out[l, core], preferred_element_type=F32).astype(BF16)
                d_out[l, first : first + group, core] = part.reshape(group, rows, width_f)
            for k in range(first, first + group):
                z = 2 * x_at(k) + my_core
                for core in range(2):
                    mine = (z == my_tp) & (my_core == core)

                    @pl.when(jnp.logical_not(mine))
                    def _(k=k, z=z, core=core):
                        src, dst = d_out.at[l, k, core], d_in.at[l, my_tp]
                        remote(src, dst, l, 3, 2 * k + core, my_tp, column(z, core)).start()

                    @pl.when(mine)
                    def _(k=k, core=core):
                        d_in[l, my_tp] = d_out[l, k, core]

        xs_t = xs.T
        for s in range(rows):
            for h in range(heads_here):
                b_row = bc[s : s + 1, 0:bw]
                xs_col = xs_t[h * hd : (h + 1) * hd, s : s + 1]
                ssm_o[l, s, h] = ssm[l, s, h] * decay[s : s + 1, h : h + 1] + xs_col * b_row
        for k in range(taps - 2):
            nx_o[l, k] = s_x[l, k + 1]
            nb_o[l, k] = s_b[l, k + 1]
            nc_o[l, k] = s_c[l, k + 1]
        nx_o[l, taps - 2] = x_new
        nb_o[l, taps - 2] = bc_new[:, 0:bw]
        nc_o[l, taps - 2] = bc_new[:, bw : 2 * bw]

        def add_d(k, total, l=l):
            z = tp_at(k)
            got = d_in.at[l, z]
            remote(got, got, l, 3, k, z, column(z, row_core)).wait_recv()
            return total + d_in[l, z].astype(F32)

        @pl.when(uneven)
        def _(l=l):
            got = d_in.at[l, my_tp]
            remote(got, got, l, 3, 0, my_tp, column(my_tp, row_core)).wait_recv()

        projected = lax.fori_loop(1, tp_n, add_d, d_in[l, my_tp].astype(F32))
        new = (r_buf[l].astype(F32) + projected).astype(BF16)
        if l + 1 < layers:
            r_buf[l + 1] = new
        else:
            res_o[...] = new

    for l in range(layers):

        def sent_a(k, carry, l=l):
            dst = a_buf.at[l, 0, my_core]
            remote(r_buf.at[l], dst, l, 0, k, 0, column(tp_at(k), row_core)).wait_send()
            return carry

        def sent_c(k, carry, l=l):
            remote(c_own.at[l], c_buf.at[l, 0], l, 2, k, 0, row(x_at(k))).wait_send()
            return carry

        def sent_parts(k, carry, l=l):
            i = rows_at(k)
            z = 2 * x_at(k) + my_core

            @pl.when(i != my_dp)
            def _():
                dst = b_in.at[l, my_x]
                remote(b_out.at[l, k], dst, l, 1, k, my_x, row(lax.div(i, 2))).wait_send()

            for core in range(2):

                @pl.when(jnp.logical_not((z == my_tp) & (my_core == core)))
                def _(core=core):
                    src, dst = d_out.at[l, k, core], d_in.at[l, my_tp]
                    remote(src, dst, l, 3, 2 * k + core, my_tp, column(z, core)).wait_send()

            return carry

        lax.fori_loop(1, tp_n, sent_a, 0)

        @pl.when(uneven)
        def _(l=l):
            dst = a_buf.at[l, 0, my_core]
            remote(r_buf.at[l], dst, l, 0, 0, my_core, column(my_tp, row_core)).wait_send()

        lax.fori_loop(1, half, sent_c, 0)
        lax.fori_loop(0, half, sent_parts, 0)
    for p in pair:
        p.wait_send()


def write_out(*refs):
    sem = refs[-1]
    half = len(refs) // 2
    copies = [
        pltpu.make_async_copy(refs[n], refs[half + n], sem.at[n]) for n in range(half)
    ]
    for c in copies:
        c.start()
    for c in copies:
        c.wait()


def body(tp_n, dp_n, *args):
    (
        tokens,
        norm_gain,
        w_z,
        w_x,
        w_b,
        w_c,
        w_dt,
        conv_x,
        conv_b,
        conv_c,
        dt_bias,
        a_log,
        d_skip,
        out_gain,
        w_out,
        ssm_state,
        state_x,
        state_b,
        state_c,
    ) = args
    layers, heads_here = dt_bias.shape
    rows, width_f = tokens.shape
    zw, bw = w_z.shape[2], w_b.shape[2]
    assert tp_n == dp_n and 2 * bw == LANES
    wide = 2 * zw + 2 * LANES
    half = tp_n // 2

    def turn(a):
        return jnp.swapaxes(a, 1, 2)

    operands = (
        tokens,
        w_z,
        w_x,
        w_out,
        norm_gain,
        turn(w_b),
        turn(w_c),
        turn(w_dt),
        conv_x,
        conv_b,
        conv_c,
        dt_bias,
        a_log,
        d_skip,
        out_gain,
        ssm_state,
        turn(state_x),
        turn(state_b),
        turn(state_c),
    )
    vmem = pl.BlockSpec(memory_space=pltpu.VMEM)
    hbm = pl.BlockSpec(memory_space=pltpu.HBM)

    def like(a):
        return pltpu.VMEM(a.shape, a.dtype)

    results = pl.pallas_call(
        functools.partial(kernel, tp_n, dp_n, width_f * dp_n),
        out_shape=(
            like(tokens),
            like(ssm_state),
            like(operands[16]),
            like(operands[17]),
            like(operands[18]),
        ),
        in_specs=[hbm] * INPUTS,
        out_specs=(vmem,) * 5,
        scratch_shapes=[
            pltpu.VMEM((layers, half, 2, rows, width_f), BF16),
            pltpu.VMEM((layers, half, rows, wide), BF16),
            pltpu.VMEM((layers, half, rows, wide), BF16),
            pltpu.VMEM((layers, rows, zw), BF16),
            pltpu.VMEM((layers, half, rows, zw), BF16),
            pltpu.VMEM((layers, half, 2, rows, width_f), BF16),
            pltpu.VMEM((layers, tp_n, rows, width_f), BF16),
            pltpu.VMEM((layers, rows, width_f), BF16),
            pltpu.VMEM((layers, 2, width_f, zw), BF16),
            pltpu.VMEM((layers, 2, width_f, zw), BF16),
            pltpu.VMEM((layers, 2, zw, width_f), BF16),
            pltpu.VMEM((layers, 2, 2 * LANES, width_f), BF16),
            pltpu.VMEM((2, 8, width_f), F32),
            pltpu.VMEM((layers, conv_x.shape[1], LANES), F32),
            pltpu.VMEM((layers, state_b.shape[2], rows, LANES), F32),
            pltpu.VMEM((layers, rows, bw, zw), BF16),
            *(pltpu.VMEM(a.shape, a.dtype) for a in operands[4:]),
            pltpu.SemaphoreType.DMA((INPUTS - 3 + 3 * layers,)),
            pltpu.SemaphoreType.DMA((2, 1 + 4 * layers)),
            pltpu.SemaphoreType.DMA((layers, 4, tp_n)),
            pltpu.SemaphoreType.DMA((layers, 4, tp_n)),
        ],
        compiler_params=pltpu.CompilerParams(
            collective_id=0, has_side_effects=True, vmem_limit_bytes=40 * 1024 * 1024
        ),
        name="decode",
    )(*(pltpu.with_memory_space_constraint(a, pltpu.HBM) for a in operands))
    results = [pltpu.with_memory_space_constraint(a, pltpu.VMEM) for a in results]
    residual, ssm_next, next_x, next_b, next_c = pl.pallas_call(
        write_out,
        out_shape=tuple(jax.ShapeDtypeStruct(a.shape, a.dtype) for a in results),
        in_specs=(vmem,) * 5,
        out_specs=(hbm,) * 5,
        scratch_shapes=[pltpu.SemaphoreType.DMA((5,))],
        compiler_params=pltpu.CompilerParams(vmem_limit_bytes=8 * 1024 * 1024),
        name="write_out",
    )(*results)
    return residual, ssm_next, turn(next_x), turn(next_b), turn(next_c)


def solution(mesh):
    placed = (
        P(("grp", "tp"), "dp"),
        P(None, "dp"),
        P(None, "dp", "tp"),
        P(None, "dp", "tp"),
        P(None, "dp", "tp"),
        P(None, "dp", "tp"),
        P(None, "dp", None),
        P(None, None, "tp"),
        P(None, None, "tp"),
        P(None, None, "tp"),
        P(None, "tp"),
        P(None, "tp"),
        P(None, "tp"),
        P(None, "tp"),
        P(None, "tp", "dp"),
        P(None, ("grp", "dp"), "tp", None, None),
        P(None, ("grp", "dp"), None, "tp"),
        P(None, ("grp", "dp"), None, "tp"),
        P(None, ("grp", "dp"), None, "tp"),
    )
    return jax.shard_map(
        functools.partial(body, mesh.shape["tp"], mesh.shape["dp"]),
        mesh=mesh,
        in_specs=placed,
        out_specs=(placed[0], placed[15], placed[16], placed[17], placed[18]),
        check_vma=False,
    )
```

time: 117 us -> 109 us (0.932)
  Pallas kernels: 116 us -> 108 us
    pallas_call x1, Pallas kernels: 114 us -> 106 us  [body(): pl.pallas_call(functools.partial(kernel, tp_n, dp_n, width_f * dp_n), out...]
where the time goes in v3:
time: 109 us
  Pallas kernels  108 us (99%)
    pallas_call x1, Pallas kernels, body(): pl.pallas_call(functools.partial(kernel, tp_n, dp_n, width_f * dp_n), out...  106 us

profile of v3, /device:TPU:65, one launch (start us, length us, event | category | flops | bytes accessed | tf_op | source)
XLA Modules:
  0.0 108.9 jit_solution(13165831390761968805)
XLA Ops:
  0.6 106.1 %decode.1 = (bf16[16,128]{1,0:T(8,128)(2,1)S(1)}, f32[2,16,4,64,64]{4,3,2,1,0:T(8,128)S(1)}, bf16[2,3,16,256]{3,2,1,0:T(8,128)(2,1)S(1)}, bf16[2,3,16,64]{3,2,1,0:T(8,128)(2,1)S(1)}, bf16[2,3,16,64]{3,2,1,0:T(8,128)(2,1)S(1)}) custom-call(bf16[16,128]{1,0:T(8,128)(2,1)} %refs_0_.1, bf16[2,128,256]{2,1,0:T(8,128)(2,1)} %refs_1_.1, ...), custom_call_target="tpu_custom_call" | custom-call | tf_op jit(solution)/shard_map/decode/pallas_call | solution.py:493
  106.8 2.1 %write_out.1 = (bf16[16,128]{1,0:T(8,128)(2,1)}, f32[2,16,4,64,64]{4,3,2,1,0:T(8,128)}, bf16[2,3,16,256]{3,2,1,0:T(8,128)(2,1)}, bf16[2,3,16,64]{3,2,1,0:T(8,128)(2,1)}, bf16[2,3,16,64]{3,2,1,0:T(8,128)(2,1)}) custom-call(bf16[16,128]{1,0:T(8,128)(2,1)S(1)} %get-tuple-element.15.refs_0_, f32[2,16,4,64,64]{4,3,2,1,0:T(8,128)S(1)} %get-tuple-element.16.refs_1_, ...), custom_call_target="tpu_custom_call" | custom-call | tf_op jit(solution)/shard_map/write_out/pallas_call | solution.py:533

commit v4 on v3

--- a/solution.py
+++ b/solution.py
@@ -62,7 +62,7 @@
     row_core = lax.rem(my_tp, 2)
 
     def nearest(k, n):
-        return jnp.where(lax.rem(k, 2) == 1, lax.div(k + 1, 2), lax.rem(n - lax.div(k, 2), n))
+        return (k + 1) // 2 if k % 2 else (n - k // 2) % n
 
     def place(distance, n):
         return jnp.where(distance <= n // 2, jnp.maximum(2 * distance - 1, 0), 2 * (n - distance))
@@ -74,16 +74,24 @@
         return lax.rem(my_x + nearest(k, half), half)
 
     def rows_at(k):
-        odd = jnp.where(lax.rem(k, 2) == 0, k + 1, tp_n - k)
+        odd = tp_n - k if k % 2 else k + 1
         return lax.rem(my_tp + jnp.where(uneven, odd, 2 * nearest(k, half)), tp_n)
 
     def rows_place(offset):
         odd = jnp.where(offset < half, offset - 1, tp_n - offset)
         return jnp.where(lax.rem(offset, 2) == 1, odd, place(lax.div(offset, 2), half))
 
+    def sent_place(k):
+        offset = (tp_n - nearest(k, tp_n)) % tp_n
+        if offset % 2:
+            return offset - 1 if offset < half else tp_n - offset
+        distance = offset // 2
+        return max(2 * distance - 1, 0) if 2 * distance <= half else 2 * (half - distance)
+
     def x_mirror(k):
-        step = jnp.where(lax.rem(k, 2) == 1, k + 1, k - 1)
-        return jnp.where((k == half - 1) & (half % 2 == 0), k, jnp.where(k == 0, 0, step))
+        if k == 0 or (k == half - 1 and half % 2 == 0):
+            return k
+        return k + 1 if k % 2 else k - 1
 
     k_rows = rows_place(lax.rem(my_dp - my_tp + tp_n, tp_n))
 
@@ -118,27 +126,83 @@
     for n in range(4, INPUTS):
         fetch.append(pltpu.make_async_copy(held[n], here[n - 4], local_sem.at[used]))
         used += 1
-    for f in fetch:
-        f.start()
+    fetch[0].start()
     barrier = pltpu.get_barrier_semaphore()
 
     def greet(device):
         pl.semaphore_signal(barrier, inc=1, device_id=device, device_id_type=MESH)
 
-    def greet_tp(k, carry):
+    for k in range(tp_n - 1, 0, -1):
         greet(column(tp_at(k), 0))
         greet(column(tp_at(k), 1))
-        return carry
-
-    def greet_dp(k, carry):
+    for k in range(half - 1, 0, -1):
         greet(row(x_at(k)))
-        return carry
-
     greet(column(my_tp, 1 - my_core))
-    lax.fori_loop(1, tp_n, greet_tp, 0)
-    lax.fori_loop(1, half, greet_dp, 0)
-
-    for f in fetch:
+    for f in fetch[1:]:
+        f.start()
+
+    def copy_a(l, k):
+        if k == 0:
+            dst = a_buf.at[l, 0, my_core]
+            return remote(r_buf.at[l], dst, l, 0, 0, my_core, column(my_tp, row_core))
+        slot = sent_place(k)
+        dst = a_buf.at[l, slot, my_core]
+        return remote(r_buf.at[l], dst, l, 0, k, 2 * slot + my_core, column(tp_at(k), row_core))
+
+    def send_a(l):
+        for k in range(tp_n - 1, 0, -1):
+            copy_a(l, k).start()
+
+        @pl.when(uneven)
+        def _():
+            copy_a(l, 0).start()
+
+        @pl.when(jnp.logical_not(uneven))
+        def _():
+            a_buf[l, 0, my_core] = r_buf[l]
+
+    def copy_b(l, k):
+        to = row(lax.div(rows_at(k), 2))
+        return remote(b_out.at[l, k], b_in.at[l, my_x], l, 1, k, my_x, to)
+
+    def copy_c(l, k):
+        slot = x_mirror(k)
+        return remote(c_own.at[l], c_buf.at[l, slot], l, 2, k, slot, row(x_at(k)))
+
+    def copy_d(l, k, core):
+        to = column(2 * x_at(k) + my_core, core)
+        return remote(d_out.at[l, k, core], d_in.at[l, my_tp], l, 3, 2 * k + core, my_tp, to)
+
+    def sent_abc(l):
+        for k in range(1, tp_n):
+            copy_a(l, k).wait_send()
+
+        @pl.when(uneven)
+        def _():
+            copy_a(l, 0).wait_send()
+
+        for k in range(half):
+
+            @pl.when(rows_at(k) != my_dp)
+            def _(k=k):
+                copy_b(l, k).wait_send()
+
+            if k > 0:
+                copy_c(l, k).wait_send()
+
+    def sent_d(l):
+        for k in range(half):
+            for core in range(2):
+
+                @pl.when(jnp.logical_not((2 * x_at(k) + my_core == my_tp) & (my_core == core)))
+                def _(k=k, core=core):
+                    copy_d(l, k, core).wait_send()
+
+    pl.semaphore_wait(barrier, 2 * tp_n - 1 + half - 1)
+    fetch[0].wait()
+    send_a(0)
+
+    for f in fetch[1:]:
         f.wait()
     heads_all = w_dtt.shape[1]
     pick = lax.broadcasted_iota(jnp.int32, (16, heads_all), 0)
@@ -160,15 +224,6 @@
     gains[my_core] = jnp.zeros(gains.shape[1:], F32)
     gains[my_core, 0:layers] = gain[...].astype(F32)
 
-    def turn(i, carry):
-        for l in range(layers):
-            block = ssm[l, i].reshape(zw, bw)
-            st_t[l, i] = block.T.astype(BF16)
-        return carry
-
-    lax.fori_loop(0, rows, turn, 0)
-    pl.semaphore_wait(barrier, 2 * tp_n - 1 + half - 1)
-
     pair = []
     for whole in [gains.at[my_core]] + [
         w.at[l, my_core] for l in layer_list for w in (w_z, w_x, w_bcd, w_out)
@@ -183,7 +238,16 @@
                 device_id_type=MESH,
             )
         )
-
+    for p in pair:
+        p.start()
+
+    def turn(i, carry):
+        for l in range(layers):
+            block = ssm[l, i].reshape(zw, bw)
+            st_t[l, i] = block.T.astype(BF16)
+        return carry
+
+    lax.fori_loop(0, rows, turn, 0)
     lane = lax.broadcasted_iota(jnp.int32, (rows, LANES), 1)
     head_of = lax.broadcasted_iota(jnp.int32, (rows, zw), 1)
     head_of = lax.div(head_of, hd)
@@ -195,28 +259,8 @@
         return out
 
     for l in range(layers):
-        def send_a(n, carry, l=l):
-            k = tp_n - 1 - n
-            z = tp_at(k)
-            slot = 2 * rows_place(lax.rem(my_tp - z + tp_n, tp_n)) + my_core
-            dst = a_buf.at[l, lax.div(slot, 2), my_core]
-            remote(r_buf.at[l], dst, l, 0, k, slot, column(z, row_core)).start()
-            return carry
-
-        lax.fori_loop(0, tp_n - 1, send_a, 0)
-
-        @pl.when(uneven)
-        def _(l=l):
-            dst = a_buf.at[l, 0, my_core]
-            remote(r_buf.at[l], dst, l, 0, 0, my_core, column(my_tp, row_core)).start()
-
-        @pl.when(jnp.logical_not(uneven))
-        def _(l=l):
-            a_buf[l, 0, my_core] = r_buf[l]
-
-        if l == 0:
-            for p in pair:
-                p.start()
+        if l > 0:
+            send_a(l)
 
         for first in range(0, half, GROUP):
             group = min(GROUP, half)
@@ -263,19 +307,16 @@
                 group, rows, LANES
             )
             for k in range(first, first + group):
-                i = rows_at(k)
-
-                @pl.when(i != my_dp)
-                def _(k=k, i=i):
-                    dst = b_in.at[l, my_x]
-                    remote(b_out.at[l, k], dst, l, 1, k, my_x, row(lax.div(i, 2))).start()
-
-        def add_b(k, total, l=l):
+
+                @pl.when(rows_at(k) != my_dp)
+                def _(k=k, l=l):
+                    copy_b(l, k).start()
+
+        total = b_out[l, k_rows].astype(F32)
+        for k in range(1, half):
             x = x_at(k)
             remote(b_in.at[l, x], b_in.at[l, x], l, 1, k, x, row(x)).wait_recv()
-            return total + b_in[l, x].astype(F32)
-
-        total = lax.fori_loop(1, half, add_b, b_out[l, k_rows].astype(F32))
+            total = total + b_in[l, x].astype(F32)
 
         small = total[:, 2 * zw + LANES :]
         small = small + pltpu.roll(small, LANES // 2, 1)
@@ -314,13 +355,8 @@
         c_own[l] = mixed
         c_buf[l, 0] = mixed
 
-        def send_c(n, carry, l=l):
-            k = half - 1 - n
-            slot = x_mirror(k)
-            remote(c_own.at[l], c_buf.at[l, slot], l, 2, k, slot, row(x_at(k))).start()
-            return carry
-
-        lax.fori_loop(0, half - 1, send_c, 0)
+        for k in range(half - 1, 0, -1):
+            copy_c(l, k).start()
 
         for first in range(0, half, GROUP):
             group = min(GROUP, half)
@@ -337,12 +373,11 @@
                     mine = (z == my_tp) & (my_core == core)
 
                     @pl.when(jnp.logical_not(mine))
-                    def _(k=k, z=z, core=core):
-                        src, dst = d_out.at[l, k, core], d_in.at[l, my_tp]
-                        remote(src, dst, l, 3, 2 * k + core, my_tp, column(z, core)).start()
+                    def _(k=k, core=core, l=l):
+                        copy_d(l, k, core).start()
 
                     @pl.when(mine)
-                    def _(k=k, core=core):
+                    def _(k=k, core=core, l=l):
                         d_in[l, my_tp] = d_out[l, k, core]
 
         xs_t = xs.T
@@ -359,62 +394,28 @@
         nb_o[l, taps - 2] = bc_new[:, 0:bw]
         nc_o[l, taps - 2] = bc_new[:, bw : 2 * bw]
 
-        def add_d(k, total, l=l):
-            z = tp_at(k)
-            got = d_in.at[l, z]
-            remote(got, got, l, 3, k, z, column(z, row_core)).wait_recv()
-            return total + d_in[l, z].astype(F32)
+        sent_abc(l)
+        if l > 0:
+            sent_d(l - 1)
 
         @pl.when(uneven)
         def _(l=l):
             got = d_in.at[l, my_tp]
             remote(got, got, l, 3, 0, my_tp, column(my_tp, row_core)).wait_recv()
 
-        projected = lax.fori_loop(1, tp_n, add_d, d_in[l, my_tp].astype(F32))
+        projected = d_in[l, my_tp].astype(F32)
+        for k in range(1, tp_n):
+            z = tp_at(k)
+            got = d_in.at[l, z]
+            remote(got, got, l, 3, k, z, column(z, row_core)).wait_recv()
+            projected = projected + d_in[l, z].astype(F32)
         new = (r_buf[l].astype(F32) + projected).astype(BF16)
         if l + 1 < layers:
             r_buf[l + 1] = new
         else:
             res_o[...] = new
 
-    for l in range(layers):
-
-        def sent_a(k, carry, l=l):
-            dst = a_buf.at[l, 0, my_core]
-            remote(r_buf.at[l], dst, l, 0, k, 0, column(tp_at(k), row_core)).wait_send()
-            return carry
-
-        def sent_c(k, carry, l=l):
-            remote(c_own.at[l], c_buf.at[l, 0], l, 2, k, 0, row(x_at(k))).wait_send()
-            return carry
-
-        def sent_parts(k, carry, l=l):
-            i = rows_at(k)
-            z = 2 * x_at(k) + my_core
-
-            @pl.when(i != my_dp)
-            def _():
-                dst = b_in.at[l, my_x]
-                remote(b_out.at[l, k], dst, l, 1, k, my_x, row(lax.div(i, 2))).wait_send()
-
-            for core in range(2):
-
-                @pl.when(jnp.logical_not((z == my_tp) & (my_core == core)))
-                def _(core=core):
-                    src, dst = d_out.at[l, k, core], d_in.at[l, my_tp]
-                    remote(src, dst, l, 3, 2 * k + core, my_tp, column(z, core)).wait_send()
-
-            return carry
-
-        lax.fori_loop(1, tp_n, sent_a, 0)
-
-        @pl.when(uneven)
-        def _(l=l):
-            dst = a_buf.at[l, 0, my_core]
-            remote(r_buf.at[l], dst, l, 0, 0, my_core, column(my_tp, row_core)).wait_send()
-
-        lax.fori_loop(1, half, sent_c, 0)
-        lax.fori_loop(0, half, sent_parts, 0)
+    sent_d(layers - 1)
     for p in pair:
         p.wait_send()
 

time: 109 us -> 108 us (level)
  no operation moved by 1% of the time
where the time goes in v4:
time: 108 us
  Pallas kernels  107 us (99%)
    pallas_call x1, Pallas kernels, body(): pl.pallas_call(functools.partial(kernel, tp_n, dp_n, width_f * dp_n), out...  105 us

profile of v4, /device:TPU:65, one launch (start us, length us, event | category | flops | bytes accessed | tf_op | source)
XLA Modules:
  0.0 108.1 jit_solution(1617105652933799339)
XLA Ops:
  0.6 105.4 %decode.1 = (bf16[16,128]{1,0:T(8,128)(2,1)S(1)}, f32[2,16,4,64,64]{4,3,2,1,0:T(8,128)S(1)}, bf16[2,3,16,256]{3,2,1,0:T(8,128)(2,1)S(1)}, bf16[2,3,16,64]{3,2,1,0:T(8,128)(2,1)S(1)}, bf16[2,3,16,64]{3,2,1,0:T(8,128)(2,1)S(1)}) custom-call(bf16[16,128]{1,0:T(8,128)(2,1)} %refs_0_.1, bf16[2,128,256]{2,1,0:T(8,128)(2,1)} %refs_1_.1, ...), custom_call_target="tpu_custom_call" | custom-call | tf_op jit(solution)/shard_map/decode/pallas_call | solution.py:494
  106.0 2.1 %write_out.1 = (bf16[16,128]{1,0:T(8,128)(2,1)}, f32[2,16,4,64,64]{4,3,2,1,0:T(8,128)}, bf16[2,3,16,256]{3,2,1,0:T(8,128)(2,1)}, bf16[2,3,16,64]{3,2,1,0:T(8,128)(2,1)}, bf16[2,3,16,64]{3,2,1,0:T(8,128)(2,1)}) custom-call(bf16[16,128]{1,0:T(8,128)(2,1)S(1)} %get-tuple-element.15.refs_0_, f32[2,16,4,64,64]{4,3,2,1,0:T(8,128)S(1)} %get-tuple-element.16.refs_1_, ...), custom_call_target="tpu_custom_call" | custom-call | tf_op jit(solution)/shard_map/write_out/pallas_call | solution.py:534

commit v5 on v4

--- a/solution.py
+++ b/solution.py
@@ -57,7 +57,7 @@
     hd = zw // heads_here
     my_tp, my_dp = lax.axis_index("tp"), lax.axis_index("dp")
     my_x, my_core = lax.div(my_dp, 2), lax.rem(my_dp, 2)
-    half = tp_n // 2
+    half, near = tp_n // 2, tp_n // 4
     uneven = lax.rem(my_tp + my_core, 2) == 1
     row_core = lax.rem(my_tp, 2)
 
@@ -132,7 +132,7 @@
     def greet(device):
         pl.semaphore_signal(barrier, inc=1, device_id=device, device_id_type=MESH)
 
-    for k in range(tp_n - 1, 0, -1):
+    for k in range(2 * near, 0, -1):
         greet(column(tp_at(k), 0))
         greet(column(tp_at(k), 1))
     for k in range(half - 1, 0, -1):
@@ -149,8 +149,11 @@
         dst = a_buf.at[l, slot, my_core]
         return remote(r_buf.at[l], dst, l, 0, k, 2 * slot + my_core, column(tp_at(k), row_core))
 
+    def reach(l):
+        return 2 * near if l == 0 else tp_n - 1
+
     def send_a(l):
-        for k in range(tp_n - 1, 0, -1):
+        for k in range(reach(l), 0, -1):
             copy_a(l, k).start()
 
         @pl.when(uneven)
@@ -161,6 +164,49 @@
         def _():
             a_buf[l, 0, my_core] = r_buf[l]
 
+    def offset_of(odd, k):
+        if odd:
+            return -k if k % 2 else k + 1
+        return -k if k % 2 == 0 else k + 1
+
+    def relayed(odd, down):
+        offsets = [offset_of(odd, k) for k in range(half)]
+        step = near if down else -near
+        return [
+            (offsets.index(o - step), k)
+            for k, o in enumerate(offsets)
+            if (o > near if down else o < -near)
+        ]
+
+    def copy_relay(source, target, down):
+        z = lax.rem(my_tp + (tp_n - near if down else near), tp_n)
+        src, dst = a_buf.at[0, source], a_buf.at[0, target]
+        return remote(src, dst, 0, 4, target, target, column(z, my_core))
+
+    def relay(odd, down):
+        for source, target in relayed(odd, down):
+            for core in range(2):
+                got = a_buf.at[0, source, core]
+                remote(
+                    got, got, 0, 0, 0, 2 * source + core, column(rows_at(source), core)
+                ).wait_recv()
+            copy_relay(source, target, down).start()
+
+    def wait_first_a(odd, k):
+        if abs(offset_of(odd, k)) > near:
+            copy_relay(k, k, 0).wait_recv()
+        elif k not in [source for down in range(2) for source, _ in relayed(odd, down)]:
+            for core in range(2):
+                got = a_buf.at[0, k, core]
+                copy = remote(got, got, 0, 0, k, 2 * k + core, column(rows_at(k), core))
+                if offset_of(odd, k) != 0:
+                    copy.wait_recv()
+                else:
+
+                    @pl.when(my_core != core)
+                    def _(copy=copy):
+                        copy.wait_recv()
+
     def copy_b(l, k):
         to = row(lax.div(rows_at(k), 2))
         return remote(b_out.at[l, k], b_in.at[l, my_x], l, 1, k, my_x, to)
@@ -174,13 +220,22 @@
         return remote(d_out.at[l, k, core], d_in.at[l, my_tp], l, 3, 2 * k + core, my_tp, to)
 
     def sent_abc(l):
-        for k in range(1, tp_n):
+        for k in range(1, reach(l) + 1):
             copy_a(l, k).wait_send()
 
         @pl.when(uneven)
         def _():
             copy_a(l, 0).wait_send()
 
+        if l == 0:
+            for odd in range(2):
+
+                @pl.when(uneven == (odd == 1))
+                def _(odd=odd):
+                    for down in range(2):
+                        for source, target in relayed(odd, down):
+                            copy_relay(source, target, down).wait_send()
+
         for k in range(half):
 
             @pl.when(rows_at(k) != my_dp)
@@ -198,7 +253,7 @@
                 def _(k=k, core=core):
                     copy_d(l, k, core).wait_send()
 
-    pl.semaphore_wait(barrier, 2 * tp_n - 1 + half - 1)
+    pl.semaphore_wait(barrier, 4 * near + 1 + half - 1)
     fetch[0].wait()
     send_a(0)
 
@@ -241,13 +296,21 @@
     for p in pair:
         p.start()
 
+    down_first = my_tp < half
+    for odd in range(2):
+        for order in ((0, 1), (1, 0)):
+
+            @pl.when((uneven == (odd == 1)) & (down_first == (order[0] == 1)))
+            def _(odd=odd, order=order):
+                for down in order:
+                    relay(odd, down)
+
     def turn(i, carry):
         for l in range(layers):
             block = ssm[l, i].reshape(zw, bw)
             st_t[l, i] = block.T.astype(BF16)
         return carry
 
-    lax.fori_loop(0, rows, turn, 0)
     lane = lax.broadcasted_iota(jnp.int32, (rows, LANES), 1)
     head_of = lax.broadcasted_iota(jnp.int32, (rows, zw), 1)
     head_of = lax.div(head_of, hd)
@@ -264,17 +327,26 @@
 
         for first in range(0, half, GROUP):
             group = min(GROUP, half)
-            for k in range(first, first + group):
-                for core in range(2):
-                    got = a_buf.at[l, k, core]
-                    copy = remote(got, got, l, 0, k, 2 * k + core, column(rows_at(k), core))
-                    if k > 0:
-                        copy.wait_recv()
-                    else:
-
-                        @pl.when(uneven | (my_core != core))
-                        def _(copy=copy):
+            if l == 0:
+                for odd in range(2):
+
+                    @pl.when(uneven == (odd == 1))
+                    def _(odd=odd, first=first, group=group):
+                        for k in range(first, first + group):
+                            wait_first_a(odd, k)
+
+            else:
+                for k in range(first, first + group):
+                    for core in range(2):
+                        got = a_buf.at[l, k, core]
+                        copy = remote(got, got, l, 0, k, 2 * k + core, column(rows_at(k), core))
+                        if k > 0:
                             copy.wait_recv()
+                        else:
+
+                            @pl.when(uneven | (my_core != core))
+                            def _(copy=copy):
+                                copy.wait_recv()
 
             if l == 0 and first == 0:
                 for p in pair:
@@ -312,6 +384,8 @@
                 def _(k=k, l=l):
                     copy_b(l, k).start()
 
+        if l == 0:
+            lax.fori_loop(0, rows, turn, 0)
         total = b_out[l, k_rows].astype(F32)
         for k in range(1, half):
             x = x_at(k)
@@ -423,9 +497,15 @@
 def write_out(*refs):
     sem = refs[-1]
     half = len(refs) // 2
-    copies = [
-        pltpu.make_async_copy(refs[n], refs[half + n], sem.at[n]) for n in range(half)
-    ]
+    copies = []
+    for n in range(half):
+        cuts = refs[n].shape[1] // 4 if len(refs[n].shape) == 5 else 0
+        for at in range(4 * refs[n].shape[0]) if cuts else (None,):
+            src, dst = refs[n], refs[half + n]
+            if cuts:
+                part = pl.ds(at % 4 * cuts, cuts)
+                src, dst = src.at[at // 4, part], dst.at[at // 4, part]
+            copies.append(pltpu.make_async_copy(src, dst, sem.at[len(copies)]))
     for c in copies:
         c.start()
     for c in copies:
@@ -522,8 +602,8 @@
             *(pltpu.VMEM(a.shape, a.dtype) for a in operands[4:]),
             pltpu.SemaphoreType.DMA((INPUTS - 3 + 3 * layers,)),
             pltpu.SemaphoreType.DMA((2, 1 + 4 * layers)),
-            pltpu.SemaphoreType.DMA((layers, 4, tp_n)),
-            pltpu.SemaphoreType.DMA((layers, 4, tp_n)),
+            pltpu.SemaphoreType.DMA((layers, 5, tp_n)),
+            pltpu.SemaphoreType.DMA((layers, 5, tp_n)),
         ],
         compiler_params=pltpu.CompilerParams(
             collective_id=0, has_side_effects=True, vmem_limit_bytes=40 * 1024 * 1024
@@ -536,7 +616,7 @@
         out_shape=tuple(jax.ShapeDtypeStruct(a.shape, a.dtype) for a in results),
         in_specs=(vmem,) * 5,
         out_specs=(hbm,) * 5,
-        scratch_shapes=[pltpu.SemaphoreType.DMA((5,))],
+        scratch_shapes=[pltpu.SemaphoreType.DMA((4 + 4 * layers,))],
         compiler_params=pltpu.CompilerParams(vmem_limit_bytes=8 * 1024 * 1024),
         name="write_out",
     )(*results)

time: 108 us -> 107 us (level)
    pallas_call x1, Pallas kernels: 105 us -> 104 us  [body(): pl.pallas_call(functools.partial(kernel, tp_n, dp_n, width_f * dp_n), out...]
where the time goes in v5:
time: 107 us
  Pallas kernels  106 us (99%)
    pallas_call x1, Pallas kernels, body(): pl.pallas_call(functools.partial(kernel, tp_n, dp_n, width_f * dp_n), out...  104 us

profile of v5, /device:TPU:65, one launch (start us, length us, event | category | flops | bytes accessed | tf_op | source)
XLA Modules:
  0.0 106.9 jit_solution(17700280938157675326)
XLA Ops:
  0.6 104.2 %decode.1 = (bf16[16,128]{1,0:T(8,128)(2,1)S(1)}, f32[2,16,4,64,64]{4,3,2,1,0:T(8,128)S(1)}, bf16[2,3,16,256]{3,2,1,0:T(8,128)(2,1)S(1)}, bf16[2,3,16,64]{3,2,1,0:T(8,128)(2,1)S(1)}, bf16[2,3,16,64]{3,2,1,0:T(8,128)(2,1)S(1)}) custom-call(bf16[16,128]{1,0:T(8,128)(2,1)} %refs_0_.1, bf16[2,128,256]{2,1,0:T(8,128)(2,1)} %refs_1_.1, ...), custom_call_target="tpu_custom_call" | custom-call | tf_op jit(solution)/shard_map/decode/pallas_call | solution.py:574
  104.8 2.1 %write_out.1 = (bf16[16,128]{1,0:T(8,128)(2,1)}, f32[2,16,4,64,64]{4,3,2,1,0:T(8,128)}, bf16[2,3,16,256]{3,2,1,0:T(8,128)(2,1)}, bf16[2,3,16,64]{3,2,1,0:T(8,128)(2,1)}, bf16[2,3,16,64]{3,2,1,0:T(8,128)(2,1)}) custom-call(bf16[16,128]{1,0:T(8,128)(2,1)S(1)} %get-tuple-element.15.refs_0_, f32[2,16,4,64,64]{4,3,2,1,0:T(8,128)S(1)} %get-tuple-element.16.refs_1_, ...), custom_call_target="tpu_custom_call" | custom-call | tf_op jit(solution)/shard_map/write_out/pallas_call | solution.py:614

commit v6 on v5

--- a/solution.py
+++ b/solution.py
@@ -32,7 +32,7 @@
     a_buf, b_out, b_in, c_own, c_buf, d_out, d_in, r_buf = refs[5:13]
     w_z, w_x, w_out, w_bcd, gains, conv_bc, s_bc, st_t = refs[13:21]
     here = refs[21 : 17 + INPUTS]
-    local_sem, pair_sem, send_sem, recv_sem = refs[17 + INPUTS :]
+    d_far, r_far, local_sem, pair_sem, send_sem, recv_sem = refs[17 + INPUTS :]
     (
         gain,
         w_bt,
@@ -149,20 +149,40 @@
         dst = a_buf.at[l, slot, my_core]
         return remote(r_buf.at[l], dst, l, 0, k, 2 * slot + my_core, column(tp_at(k), row_core))
 
-    def reach(l):
-        return 2 * near if l == 0 else tp_n - 1
-
-    def send_a(l):
-        for k in range(reach(l), 0, -1):
-            copy_a(l, k).start()
+    def copy_a2(l, n):
+        steps = [(s, False) for s in range(-near, near + 1)]
+        steps += [(s, True) for s in range(1 - near, near)]
+        s, far = steps[n]
+        offset = -s if not far else (half - s if s >= 0 else -half - s)
+        slot = offset - 1 if offset > 0 else -offset
+        src = r_far.at[1] if far else r_buf.at[l]
+        dst = a_buf.at[l, slot, my_core]
+        to = column(lax.rem(my_tp + s + tp_n, tp_n), row_core)
+        return s, remote(src, dst, l, 0, n, 2 * slot + my_core, to)
+
+    def each_a(l, act):
+        if l == 0:
+            copies = [(k, copy_a(l, k)) for k in range(2 * near, -1, -1)]
+        else:
+            copies = [copy_a2(l, n) for n in range(tp_n)]
+        for s, copy in copies:
+            if s != 0:
+                act(copy)
 
         @pl.when(uneven)
         def _():
-            copy_a(l, 0).start()
+            for s, copy in copies:
+                if s == 0:
+                    act(copy)
+
+    def send_a(l):
+        each_a(l, lambda copy: copy.start())
 
         @pl.when(jnp.logical_not(uneven))
         def _():
             a_buf[l, 0, my_core] = r_buf[l]
+            if l > 0:
+                a_buf[l, half - 1, my_core] = r_far[1]
 
     def offset_of(odd, k):
         if odd:
@@ -219,13 +239,17 @@
         to = column(2 * x_at(k) + my_core, core)
         return remote(d_out.at[l, k, core], d_in.at[l, my_tp], l, 3, 2 * k + core, my_tp, to)
 
+    def copy_d2(l, k, core):
+        z = lax.rem(2 * x_at(k) + my_core + half, tp_n)
+        src, dst = d_out.at[l, k, core], d_far.at[my_tp]
+        return z, remote(src, dst, l, 5, 2 * k + core, my_tp, column(z, core))
+
+    def copy_far():
+        src = a_buf.at[0, half - 1, 1 - my_core]
+        return remote(src, r_far.at[0], 0, 6, 0, 0, column(my_tp, 1 - my_core))
+
     def sent_abc(l):
-        for k in range(1, reach(l) + 1):
-            copy_a(l, k).wait_send()
-
-        @pl.when(uneven)
-        def _():
-            copy_a(l, 0).wait_send()
+        each_a(l, lambda copy: copy.wait_send())
 
         if l == 0:
             for odd in range(2):
@@ -252,6 +276,13 @@
                 @pl.when(jnp.logical_not((2 * x_at(k) + my_core == my_tp) & (my_core == core)))
                 def _(k=k, core=core):
                     copy_d(l, k, core).wait_send()
+
+                if l + 1 < layers:
+                    z, copy = copy_d2(l, k, core)
+
+                    @pl.when(jnp.logical_not((z == my_tp) & (my_core == core)))
+                    def _(copy=copy):
+                        copy.wait_send()
 
     pl.semaphore_wait(barrier, 4 * near + 1 + half - 1)
     fetch[0].wait()
@@ -340,7 +371,7 @@
                     for core in range(2):
                         got = a_buf.at[l, k, core]
                         copy = remote(got, got, l, 0, k, 2 * k + core, column(rows_at(k), core))
-                        if k > 0:
+                        if k not in (0, half - 1):
                             copy.wait_recv()
                         else:
 
@@ -385,6 +416,12 @@
                     copy_b(l, k).start()
 
         if l == 0:
+
+            @pl.when(jnp.logical_not(uneven))
+            def _():
+                copy_far().start()
+                r_far[0] = a_buf[0, half - 1, my_core]
+
             lax.fori_loop(0, rows, turn, 0)
         total = b_out[l, k_rows].astype(F32)
         for k in range(1, half):
@@ -454,6 +491,18 @@
                     def _(k=k, core=core, l=l):
                         d_in[l, my_tp] = d_out[l, k, core]
 
+                    if l + 1 < layers:
+                        z2, copy = copy_d2(l, k, core)
+                        mine2 = (z2 == my_tp) & (my_core == core)
+
+                        @pl.when(jnp.logical_not(mine2))
+                        def _(copy=copy):
+                            copy.start()
+
+                        @pl.when(mine2)
+                        def _(k=k, core=core, l=l):
+                            d_far[my_tp] = d_out[l, k, core]
+
         xs_t = xs.T
         for s in range(rows):
             for h in range(heads_here):
@@ -486,6 +535,24 @@
         new = (r_buf[l].astype(F32) + projected).astype(BF16)
         if l + 1 < layers:
             r_buf[l + 1] = new
+
+            @pl.when(uneven)
+            def _(l=l):
+                copy_far().wait_recv()
+                got = d_far.at[my_tp]
+                remote(got, got, l, 5, 0, my_tp, column(my_tp, row_core)).wait_recv()
+
+            @pl.when(jnp.logical_not(uneven))
+            def _():
+                copy_far().wait_send()
+
+            projected = d_far[my_tp].astype(F32)
+            for k in range(1, tp_n):
+                z = tp_at(k)
+                got = d_far.at[z]
+                remote(got, got, l, 5, k, z, column(z, row_core)).wait_recv()
+                projected = projected + d_far[z].astype(F32)
+            r_far[1] = (r_far[0].astype(F32) + projected).astype(BF16)
         else:
             res_o[...] = new
 
@@ -537,7 +604,7 @@
     layers, heads_here = dt_bias.shape
     rows, width_f = tokens.shape
     zw, bw = w_z.shape[2], w_b.shape[2]
-    assert tp_n == dp_n and 2 * bw == LANES
+    assert tp_n == dp_n and layers == 2 and tp_n % 8 == 0 and 2 * bw == LANES
     wide = 2 * zw + 2 * LANES
     half = tp_n // 2
 
@@ -600,10 +667,12 @@
             pltpu.VMEM((layers, state_b.shape[2], rows, LANES), F32),
             pltpu.VMEM((layers, rows, bw, zw), BF16),
             *(pltpu.VMEM(a.shape, a.dtype) for a in operands[4:]),
+            pltpu.VMEM((tp_n, rows, width_f), BF16),
+            pltpu.VMEM((2, rows, width_f), BF16),
             pltpu.SemaphoreType.DMA((INPUTS - 3 + 3 * layers,)),
             pltpu.SemaphoreType.DMA((2, 1 + 4 * layers)),
-            pltpu.SemaphoreType.DMA((layers, 5, tp_n)),
-            pltpu.SemaphoreType.DMA((layers, 5, tp_n)),
+            pltpu.SemaphoreType.DMA((layers, 7, tp_n)),
+            pltpu.SemaphoreType.DMA((layers, 7, tp_n)),
         ],
         compiler_params=pltpu.CompilerParams(
             collective_id=0, has_side_effects=True, vmem_limit_bytes=40 * 1024 * 1024

time: 107 us -> 108 us (level)
  no operation moved by 1% of the time
where the time goes in v6:
time: 108 us
  Pallas kernels  107 us (99%)
    pallas_call x1, Pallas kernels, body(): pl.pallas_call(functools.partial(kernel, tp_n, dp_n, width_f * dp_n), out...  105 us

profile of v6, /device:TPU:65, one launch (start us, length us, event | category | flops | bytes accessed | tf_op | source)
XLA Modules:
  0.0 108.0 jit_solution(3679752090087294985)
XLA Ops:
  0.6 105.2 %decode.1 = (bf16[16,128]{1,0:T(8,128)(2,1)S(1)}, f32[2,16,4,64,64]{4,3,2,1,0:T(8,128)S(1)}, bf16[2,3,16,256]{3,2,1,0:T(8,128)(2,1)S(1)}, bf16[2,3,16,64]{3,2,1,0:T(8,128)(2,1)S(1)}, bf16[2,3,16,64]{3,2,1,0:T(8,128)(2,1)S(1)}) custom-call(bf16[16,128]{1,0:T(8,128)(2,1)} %refs_0_.1, bf16[2,128,256]{2,1,0:T(8,128)(2,1)} %refs_1_.1, ...), custom_call_target="tpu_custom_call" | custom-call | tf_op jit(solution)/shard_map/decode/pallas_call | solution.py:641
  105.8 2.1 %write_out.1 = (bf16[16,128]{1,0:T(8,128)(2,1)}, f32[2,16,4,64,64]{4,3,2,1,0:T(8,128)}, bf16[2,3,16,256]{3,2,1,0:T(8,128)(2,1)}, bf16[2,3,16,64]{3,2,1,0:T(8,128)(2,1)}, bf16[2,3,16,64]{3,2,1,0:T(8,128)(2,1)}) custom-call(bf16[16,128]{1,0:T(8,128)(2,1)S(1)} %get-tuple-element.15.refs_0_, f32[2,16,4,64,64]{4,3,2,1,0:T(8,128)S(1)} %get-tuple-element.16.refs_1_, ...), custom_call_target="tpu_custom_call" | custom-call | tf_op jit(solution)/shard_map/write_out/pallas_call | solution.py:683

commit v7 on v5

--- a/solution.py
+++ b/solution.py
@@ -14,7 +14,7 @@
 NT = (((1,), (1,)), ((), ()))
 LANES = 128
 INPUTS = 19
-GROUP = 4
+GROUP = 2
 
 
 def silu(v):

time: 107 us -> 106 us (level)
    pallas_call x1, Pallas kernels: 104 us -> 103 us  [body(): pl.pallas_call(functools.partial(kernel, tp_n, dp_n, width_f * dp_n), out...]
where the time goes in v7:
time: 106 us; the launch traced here: 105 us
  Pallas kernels  105 us (99%)
    pallas_call x1, Pallas kernels, body(): pl.pallas_call(functools.partial(kernel, tp_n, dp_n, width_f * dp_n), out...  103 us
    pallas_call x1, Pallas kernels, body(): pl.pallas_call(write_out, out_shape=tuple((jax.ShapeDtypeStruct(a.shape,...  2.12 us

profile of v7, /device:TPU:65, one launch (start us, length us, event | category | flops | bytes accessed | tf_op | source)
XLA Modules:
  0.0 105.4 jit_solution(18031598567675685340)
XLA Ops:
  0.6 102.6 %decode.1 = (bf16[16,128]{1,0:T(8,128)(2,1)S(1)}, f32[2,16,4,64,64]{4,3,2,1,0:T(8,128)S(1)}, bf16[2,3,16,256]{3,2,1,0:T(8,128)(2,1)S(1)}, bf16[2,3,16,64]{3,2,1,0:T(8,128)(2,1)S(1)}, bf16[2,3,16,64]{3,2,1,0:T(8,128)(2,1)S(1)}) custom-call(bf16[16,128]{1,0:T(8,128)(2,1)} %refs_0_.1, bf16[2,128,256]{2,1,0:T(8,128)(2,1)} %refs_1_.1, ...), custom_call_target="tpu_custom_call" | custom-call | tf_op jit(solution)/shard_map/decode/pallas_call | solution.py:574
  103.3 2.1 %write_out.1 = (bf16[16,128]{1,0:T(8,128)(2,1)}, f32[2,16,4,64,64]{4,3,2,1,0:T(8,128)}, bf16[2,3,16,256]{3,2,1,0:T(8,128)(2,1)}, bf16[2,3,16,64]{3,2,1,0:T(8,128)(2,1)}, bf16[2,3,16,64]{3,2,1,0:T(8,128)(2,1)}) custom-call(bf16[16,128]{1,0:T(8,128)(2,1)S(1)} %get-tuple-element.15.refs_0_, f32[2,16,4,64,64]{4,3,2,1,0:T(8,128)S(1)} %get-tuple-element.16.refs_1_, ...), custom_call_target="tpu_custom_call" | custom-call | tf_op jit(solution)/shard_map/write_out/pallas_call | solution.py:614

commit v8 on v7

--- a/solution.py
+++ b/solution.py
@@ -14,7 +14,7 @@
 NT = (((1,), (1,)), ((), ()))
 LANES = 128
 INPUTS = 19
-GROUP = 2
+GROUP = 1
 
 
 def silu(v):

time: 106 us -> 104 us (0.981)
  the two profiles are of different devices: /device:TPU:65 before, /device:TPU:83 now
where the time goes in v8:
time: 104 us
  Pallas kernels  103 us (99%)
    pallas_call x1, Pallas kernels, body(): pl.pallas_call(functools.partial(kernel, tp_n, dp_n, width_f * dp_n), out...  101 us
    pallas_call x1, Pallas kernels, body(): pl.pallas_call(write_out, out_shape=tuple((jax.ShapeDtypeStruct(a.shape,...  2.12 us

profile of v8, /device:TPU:83, one launch (start us, length us, event | category | flops | bytes accessed | tf_op | source)
XLA Modules:
  0.0 103.9 jit_solution(2474265803343838827)
XLA Ops:
  0.6 101.2 %decode.1 = (bf16[16,128]{1,0:T(8,128)(2,1)S(1)}, f32[2,16,4,64,64]{4,3,2,1,0:T(8,128)S(1)}, bf16[2,3,16,256]{3,2,1,0:T(8,128)(2,1)S(1)}, bf16[2,3,16,64]{3,2,1,0:T(8,128)(2,1)S(1)}, bf16[2,3,16,64]{3,2,1,0:T(8,128)(2,1)S(1)}) custom-call(bf16[16,128]{1,0:T(8,128)(2,1)} %refs_0_.1, bf16[2,128,256]{2,1,0:T(8,128)(2,1)} %refs_1_.1, ...), custom_call_target="tpu_custom_call" | custom-call | tf_op jit(solution)/shard_map/decode/pallas_call | solution.py:574
  101.8 2.1 %write_out.1 = (bf16[16,128]{1,0:T(8,128)(2,1)}, f32[2,16,4,64,64]{4,3,2,1,0:T(8,128)}, bf16[2,3,16,256]{3,2,1,0:T(8,128)(2,1)}, bf16[2,3,16,64]{3,2,1,0:T(8,128)(2,1)}, bf16[2,3,16,64]{3,2,1,0:T(8,128)(2,1)}) custom-call(bf16[16,128]{1,0:T(8,128)(2,1)S(1)} %get-tuple-element.15.refs_0_, f32[2,16,4,64,64]{4,3,2,1,0:T(8,128)S(1)} %get-tuple-element.16.refs_1_, ...), custom_call_target="tpu_custom_call" | custom-call | tf_op jit(solution)/shard_map/write_out/pallas_call | solution.py:614

commit v9 on v6

--- a/solution.py
+++ b/solution.py
@@ -14,7 +14,7 @@
 NT = (((1,), (1,)), ((), ()))
 LANES = 128
 INPUTS = 19
-GROUP = 4
+GROUP = 1
 
 
 def silu(v):

time: 108 us -> 105 us (0.972); the launches traced: 108 us -> 103 us
  Pallas kernels: 107 us -> 102 us
    pallas_call x1, Pallas kernels: 105 us -> 100 us  [body(): pl.pallas_call(functools.partial(kernel, tp_n, dp_n, width_f * dp_n), out...]
where the time goes in v9:
time: 105 us; the launch traced here: 103 us
  Pallas kernels  102 us (97%)
    pallas_call x1, Pallas kernels, body(): pl.pallas_call(functools.partial(kernel, tp_n, dp_n, width_f * dp_n), out...  100 us
    pallas_call x1, Pallas kernels, body(): pl.pallas_call(write_out, out_shape=tuple((jax.ShapeDtypeStruct(a.shape,...  2.12 us

profile of v9, /device:TPU:65, one launch (start us, length us, event | category | flops | bytes accessed | tf_op | source)
XLA Modules:
  0.0 103.0 jit_solution(4938806840754269155)
XLA Ops:
  0.6 100.2 %decode.1 = (bf16[16,128]{1,0:T(8,128)(2,1)S(1)}, f32[2,16,4,64,64]{4,3,2,1,0:T(8,128)S(1)}, bf16[2,3,16,256]{3,2,1,0:T(8,128)(2,1)S(1)}, bf16[2,3,16,64]{3,2,1,0:T(8,128)(2,1)S(1)}, bf16[2,3,16,64]{3,2,1,0:T(8,128)(2,1)S(1)}) custom-call(bf16[16,128]{1,0:T(8,128)(2,1)} %refs_0_.1, bf16[2,128,256]{2,1,0:T(8,128)(2,1)} %refs_1_.1, ...), custom_call_target="tpu_custom_call" | custom-call | tf_op jit(solution)/shard_map/decode/pallas_call | solution.py:641
  100.9 2.1 %write_out.1 = (bf16[16,128]{1,0:T(8,128)(2,1)}, f32[2,16,4,64,64]{4,3,2,1,0:T(8,128)}, bf16[2,3,16,256]{3,2,1,0:T(8,128)(2,1)}, bf16[2,3,16,64]{3,2,1,0:T(8,128)(2,1)}, bf16[2,3,16,64]{3,2,1,0:T(8,128)(2,1)}) custom-call(bf16[16,128]{1,0:T(8,128)(2,1)S(1)} %get-tuple-element.15.refs_0_, f32[2,16,4,64,64]{4,3,2,1,0:T(8,128)S(1)} %get-tuple-element.16.refs_1_, ...), custom_call_target="tpu_custom_call" | custom-call | tf_op jit(solution)/shard_map/write_out/pallas_call | solution.py:683
